TPU v7x, 512 devices: a whole 4x4x16 slice. The times are simulated.
512 devices in a mesh: ep: 32 (over z, core), tp: 16 (over y, x).
Axes of the slice: x: 4, y: 4, z: 16, core: 2. Of those that a mesh axis runs over, the one named last changes fastest.
Arguments:
- attn_in: bfloat16 [16384, 2048], P('ep'), may hold values from -6 to 6
- mix_gain: float32 [2048], replicated, may hold values from 0.1 to 1.9
- query_weight: bfloat16 [2048, 1024], P(None, 'tp'), may hold values from -0.125 to 0.125
- key_weight: bfloat16 [2048, 1024], P(None, 'tp'), may hold values from -0.125 to 0.125
- value_weight: bfloat16 [2048, 1024], P(None, 'tp'), may hold values from -0.125 to 0.125
- query_gain: float32 [64], replicated, may hold values from 0.7 to 6
- key_gain: float32 [64], replicated, may hold values from 0.7 to 6
- log_cache: float32 [16384, 16], P('ep', 'tp'), as said below
- head_gain: float32 [1024], P('tp'), may hold values from 0.1 to 1.9
- out_weight: bfloat16 [1024, 2048], P(None, 'tp'), may hold values from -0.1875 to 0.1875
- moe_in: bfloat16 [4096, 2048], P('ep'), may hold values from -6 to 6
- moe_gain: float32 [2048], replicated, may hold values from 0.1 to 1.9
- routes: int32 [4096, 2], P('ep'), may hold values from 0 to 31, all different within a row; in each aligned block of 128 rows (0 to 127, 128 to 255, ...) at most 12 rows name the same one
- route_weight: float32 [4096, 2], P('ep'), may hold values from 0.25 to 1
- expert_gate: bfloat16 [32, 2048, 1024], P('ep', None, 'tp'), may hold values from -0.125 to 0.125
- expert_up: bfloat16 [32, 2048, 1024], P('ep', None, 'tp'), may hold values from -0.125 to 0.125
- expert_down: bfloat16 [32, 1024, 2048], P('ep', 'tp'), may hold values from -0.1875 to 0.1875
Outputs:
- mixer_out: bfloat16 [16384, 2048], P('ep', 'tp')
- moe_out: bfloat16 [4096, 2048], P('ep', 'tp')
Inputs may be any that keep to these rules, and one draw needn't show every extreme that they name: `routes`: each row names 2 different experts; within the rows of one index of ep (aligned blocks of 128 rows) no expert is named by more than 12 rows. `log_cache`: never increasing along positions for each head.
All inputs are finite; a program needn't handle non-finite values.
Results may differ from a plain program's by a relative error of at most 0.015.
The roundings to bfloat16 on the way count: a program that leaves them out, or rounds other values in their place, can miss the bound.
Values may be sent and summed in bfloat16 or wider, within the bound.
A program may use at most 64 MiB of HBM per device.

v0:
```python
import math

import jax
import jax.numpy as jnp
from jax import lax
from jax.sharding import PartitionSpec as P

HD = 64


epsilon = 1e-06


def sent_together(arrays, axis, dim, along):
    widths = [a.shape[along] for a in arrays]
    both = jnp.concatenate(arrays, axis=along)
    whole = lax.all_gather(both, axis, axis=dim, tiled=True)
    return tuple(jnp.split(whole, [sum(widths[:k]) for k in range(1, len(widths))], axis=along))


def laid_out(tiles, dim):
    lengths = list(tiles.shape[1:])
    lengths[dim] *= tiles.shape[0]
    return jnp.moveaxis(tiles, 0, dim).reshape(lengths)


def from_everyone(value, axis):
    length = lax.axis_size(axis)
    return lax.all_to_all(
        jnp.broadcast_to(value[None], (length, *value.shape)), axis, 0, 0, tiled=True
    )


def collect(value, axis, dim):
    return laid_out(from_everyone(value, axis), dim)


def split_up(value, dim, length):
    before, after = (value.shape[:dim], value.shape[dim + 1 :])
    return jnp.moveaxis(value.reshape(*before, length, -1, *after), dim, 0)


def sent_and_summed(value, axis, dim):
    tiles = split_up(value, dim, lax.axis_size(axis))
    arrived = lax.all_to_all(tiles, axis, split_axis=0, concat_axis=0, tiled=True)
    return arrived.astype(jnp.float32).sum(axis=0)


def row_norm(inputs, gain_vec):
    floats = inputs.astype(jnp.float32)
    scaled = floats * lax.rsqrt(jnp.mean(floats * floats, axis=-1, keepdims=True) + epsilon)
    return scaled * gain_vec


def body(
    attn_in,
    mix_gain,
    query_weight,
    key_weight,
    value_weight,
    query_gain,
    key_gain,
    log_cache,
    head_gain,
    out_weight,
    moe_in,
    moe_gain,
    routes,
    route_weight,
    expert_gate,
    expert_up,
    expert_down,
):
    tok_rows = attn_in.shape[0]
    local_heads = query_weight.shape[1] // HD
    normed = row_norm(attn_in, mix_gain).astype(jnp.bfloat16)

    def project(weight):
        return jnp.dot(normed, weight, preferred_element_type=jnp.float32).reshape(
            tok_rows, local_heads, HD
        )

    queries = row_norm(project(query_weight), query_gain).astype(jnp.bfloat16)
    key_rows = (
        row_norm(project(key_weight), key_gain)
        .astype(jnp.bfloat16)
        .reshape(tok_rows, local_heads * HD)
    )
    value_rows = project(value_weight).astype(jnp.bfloat16).reshape(tok_rows, local_heads * HD)
    all_gates = lax.all_gather(log_cache, "ep", axis=0, tiled=True)
    query_pos = lax.axis_index("ep") * tok_rows + jnp.arange(tok_rows, dtype=jnp.int32)
    query_gates = jnp.transpose(log_cache)[:, :, None]
    score_scale = HD ** (-0.5)
    init_state = (
        jnp.full((local_heads, tok_rows), -1e30, jnp.float32),
        jnp.zeros((local_heads, tok_rows), jnp.float32),
        jnp.zeros((local_heads, tok_rows, HD), jnp.float32),
    )
    key_piece, value_piece = sent_together((key_rows, value_rows), "ep", 0, 1)
    span_len = key_piece.shape[0]
    block_len = math.gcd(span_len, 512)

    def block_step(block_index, running):
        running_max, running_sum, weighted = running
        block_begin = block_index * block_len
        key_block = lax.dynamic_slice_in_dim(key_piece, block_begin, block_len, 0).reshape(
            block_len, local_heads, HD
        )
        value_block = lax.dynamic_slice_in_dim(value_piece, block_begin, block_len, 0).reshape(
            block_len, local_heads, HD
        )
        gate_block = lax.dynamic_slice_in_dim(all_gates, block_begin, block_len, 0)
        scores = (
            jnp.einsum("qhd,khd->hqk", queries, key_block, preferred_element_type=jnp.float32)
            * score_scale
        )
        scores = scores + query_gates - jnp.transpose(gate_block)[:, None, :]
        key_pos = block_begin + jnp.arange(block_len, dtype=jnp.int32)
        causal = (key_pos[None, :] <= query_pos[:, None])[None]
        new_max = jnp.maximum(running_max, jnp.max(jnp.where(causal, scores, -1e30), axis=2))
        expo_scores = jnp.where(causal, jnp.exp(scores - new_max[:, :, None]), 0.0)
        rescale = jnp.exp(running_max - new_max)
        running_sum = running_sum * rescale + jnp.sum(expo_scores, axis=2)
        weighted = weighted * rescale[:, :, None] + jnp.einsum(
            "hqk,khd->hqd",
            expo_scores.astype(jnp.bfloat16),
            value_block,
            preferred_element_type=jnp.float32,
        )
        return (new_max, running_sum, weighted)

    final_max, final_sum, weighted = lax.fori_loop(0, span_len // block_len, block_step, init_state)
    attended = jnp.transpose(weighted / final_sum[:, :, None], (1, 0, 2))
    head_out = (
        row_norm(attended, head_gain.reshape(local_heads, HD))
        .astype(jnp.bfloat16)
        .reshape(tok_rows, local_heads * HD)
    )
    mixer_out = jnp.dot(
        collect(head_out, "tp", 1), out_weight, preferred_element_type=jnp.float32
    ).astype(jnp.bfloat16)
    moe_rows = moe_in.shape[0]
    top_count = routes.shape[1]
    local_experts = expert_gate.shape[0]
    senders = lax.axis_size("ep")
    expert_count = local_experts * senders
    capacity = 3 * moe_rows * top_count // (2 * expert_count)
    model_width = moe_in.shape[1]
    moe_normed = row_norm(moe_in, moe_gain).astype(jnp.bfloat16)
    flat_routes = routes.reshape(-1)
    one_hot = (flat_routes[:, None] == jnp.arange(expert_count, dtype=jnp.int32)[None, :]).astype(
        jnp.int32
    )
    order_in = jnp.sum(jnp.cumsum(one_hot, axis=0) * one_hot, axis=1) - 1
    slot_index = flat_routes * capacity + order_in
    token_of = jnp.arange(flat_routes.shape[0], dtype=jnp.int32) // top_count
    source_row = jnp.zeros((expert_count * capacity,), jnp.int32).at[slot_index].set(token_of)
    filled = jnp.zeros((expert_count * capacity,), jnp.bool_).at[slot_index].set(True)
    send_buffer = jnp.where(
        filled[:, None], moe_normed[source_row], jnp.zeros((), jnp.bfloat16)
    ).reshape(expert_count, capacity, model_width)
    share_width = model_width // lax.axis_size("tp")
    share_part = lax.dynamic_slice_in_dim(
        send_buffer, lax.axis_index("tp") * share_width, share_width, 2
    )
    arrived = lax.all_to_all(share_part, "ep", split_axis=0, concat_axis=0, tiled=True)
    piece_now = collect(arrived, "tp", 2)
    piece_cols = piece_now.shape[2]
    piece_rows = piece_now.reshape(senders, local_experts, capacity, piece_cols)
    gate_next = jnp.einsum(
        "sjcd,jdf->sjcf", piece_rows, expert_gate, preferred_element_type=jnp.float32
    )
    up_next = jnp.einsum(
        "sjcd,jdf->sjcf", piece_rows, expert_up, preferred_element_type=jnp.float32
    )
    hidden = (jax.nn.silu(gate_next) * up_next).astype(jnp.bfloat16)
    partial_value = jnp.einsum(
        "sjcf,jfd->sjcd", hidden, expert_down, preferred_element_type=jnp.float32
    )
    summed = sent_and_summed(partial_value.astype(jnp.bfloat16), "tp", 3).astype(jnp.bfloat16)
    out_cols = summed.shape[3]
    returned = lax.all_to_all(
        summed.reshape(expert_count, capacity, out_cols),
        "ep",
        split_axis=0,
        concat_axis=0,
        tiled=True,
    )
    picked = returned.reshape(expert_count * capacity, out_cols)[slot_index].astype(jnp.float32)
    weighted_rows = picked * route_weight.reshape(-1)[:, None]
    moe_out = jnp.sum(weighted_rows.reshape(moe_rows, top_count, out_cols), axis=1).astype(
        jnp.bfloat16
    )
    return (mixer_out, moe_out)


def solution(mesh):
    in_specs = (
        P("ep", None),
        P(),
        P(None, "tp"),
        P(None, "tp"),
        P(None, "tp"),
        P(),
        P(),
        P("ep", "tp"),
        P("tp"),
        P(None, "tp"),
        P("ep", None),
        P(),
        P("ep", None),
        P("ep", None),
        P("ep", None, "tp"),
        P("ep", None, "tp"),
        P("ep", "tp", None),
    )
    out_specs = (P("ep", "tp"), P("ep", "tp"))
    return jax.shard_map(body, mesh=mesh, in_specs=in_specs, out_specs=out_specs, check_vma=False)
```

profile of v0, /device:TPU:1, one launch (start us, length us, event | category | flops | bytes accessed | tf_op | source)
XLA Modules:
  0.0 239.5 jit_solution(8598597229880159288)
XLA Ops:
  7.2 2.2 fusion.23
  9.5 1.3 fusion.25
  15.0 1.4 scatter_custom_fusion.1
  16.4 1.5 scatter_custom_fusion
  18.4 3.1 %gather_fusion = bf16[384,2048]{1,0:T(8,128)(2,1)} fusion(bf16[128,2048]{1,0:T(8,128)(2,1)S(1)} %fusion.50, s32[1024]{0:T(1024)S(1)} %pad_clamp_fusion.1), kind=kCustom, calls=%fused_computation | custom fusion | bytes 3147264 | tf_op jit(solution)/shard_map/gather | solution.py:160
  21.5 3.6 %gather.9 = bf16[32,12,2048]{2,1,0:T(8,128)(2,1)} reshape(bf16[384,2048]{1,0:T(8,128)(2,1)} %gather_fusion) | data formatting | bytes 3145728 | tf_op jit(solution)/shard_map/gather | solution.py:160
  26.2 34.5 %all_to_all.25 = bf16[32,12,128]{2,1,0:T(8,128)(2,1)S(1)} all-to-all(bf16[32,12,128]{2,1,0:T(8,128)(2,1)S(1)} %dynamic-slice_select_fusion), channel_id=1, replica_groups=mesh['ep'=32,'tp'=16] {'ep'}, dimensions={0} | all-to-all | bytes 196608 | tf_op jit(solution)/shard_map/all_to_all | solution.py:166
  61.1 28.8 %all_to_all.26 = bf16[16,32,12,128]{3,1,2,0:T(8,128)(2,1)S(1)} all-to-all(bf16[16,32,12,128]{3,1,2,0:T(8,128)(2,1)S(1)} %broadcast_in_dim.97), channel_id=1, replica_groups=mesh['ep'=32,'tp'=16] {'tp'}, dimensions={0} | all-to-all | bytes 3145728 | tf_op jit(solution)/shard_map/all_to_all | solution.py:29
  92.0 4.4 %fusion.30 = bf16[1,12,4,16,8,128]{5,4,3,2,1,0:T(8,128)(2,1)} fusion(bf16[1,64,2048]{2,1,0:T(8,128)(2,1)S(1)} %copy-done, bf16[1,2048,64]{1,2,0:T(8,128)(2,1)S(1)} %copy-done.8, f32[32,1,12,64]{3,0,2,1:T(8,128)S(1)} %fusion.33, bf16[16,32,12,128]{3,1,2,0:T(8,128)(2,1)} %copy-done.2), kind=kOutput, calls=%fused_computation.47 | convolution fusion | flops 202260480 | bytes 3768320 | tf_op jit(solution)/shard_map/sjcf,jfd->sjcd/dot_general | solution.py:177
  96.4 3.0 %copy.85 = bf16[1,12,4,16,8,128]{5,4,2,1,0,3:T(8,128)(2,1)} copy(bf16[1,12,4,16,8,128]{5,4,3,2,1,0:T(8,128)(2,1)} %fusion.30) | data formatting | bytes 3145728 | tf_op jit(solution)/shard_map/reshape | solution.py:40
  99.4 4.5 %all-to-all-start.3 = ((bf16[16,32,1,12,128]{4,1,3,2,0:T(8,128)(2,1)}), bf16[16,32,1,12,128]{4,1,3,2,0:T(8,128)(2,1)}, u32[]{:S(2)}, u32[]{:S(2)}) async-start(bf16[16,32,1,12,128]{4,1,3,2,0:T(8,128)(2,1)} %bitcast.147), calls=%async_computation.3 | async-start | bytes 3145728 | tf_op jit(solution)/shard_map/all_to_all | solution.py:45
  104.0 28.7 %all_gather.7 = f32[16384,1]{0,1:T(1,128)S(1)} all-gather(f32[512,1]{0,1:T(1,128)S(1)} %copy-done.11), channel_id=1, replica_groups=mesh['ep'=32,'tp'=16] {'ep'}, dimensions={0}, use_global_device_ids=true | all-gather | bytes 67584 | tf_op jit(solution)/shard_map/all_gather | solution.py:90
  133.5 1.6 reduce_sum.94
  135.8 4.4 %all-to-all-start.4 = ((bf16[32,12,128]{2,1,0:T(8,128)(2,1)}), bf16[32,12,128]{2,1,0:T(8,128)(2,1)S(1)}, u32[]{:S(2)}, u32[]{:S(2)}) async-start(bf16[32,12,128]{2,1,0:T(8,128)(2,1)} %copy.55), calls=%async_computation.4 | async-start | bytes 262144 | tf_op jit(solution)/shard_map/all_to_all | solution.py:182
  140.2 3.9 %fusion.74 = (bf16[16384,64]{0,1:T(8,128)(2,1)S(1)}, bf16[16384,64]{0,1:T(8,128)(2,1)}) fusion(bf16[16384,128]{0,1:T(8,128)(2,1)} %all-gather.2.cloned.1.call-done), kind=kLoop, calls=%fused_computation.112 | loop fusion | bytes 8388608 | tf_op jit(solution)/shard_map/split | solution.py:18
  144.1 63.1 %while.18 = (s32[]{:T(128)}, f32[1,512]{1,0:T(1,128)S(1)}, f32[1,512]{1,0:T(1,128)S(1)}, f32[1,512,64]{1,2,0:T(8,128)S(1)}, bf16[16384,64]{0,1:T(8,128)(2,1)}, /...) while((s32[]{:T(128)}, f32[1,512]{1,0:T(1,128)S(1)}, ...), condition=%wide.region_6.7_spmd.clone, body=%wide.region_3.6_spmd.clone.sunk | while | flops 70880768 | bytes 3662043 | solution.py:132
  144.1 1.3 fusion.94
  146.1 1.3 fusion.94
  148.1 1.3 fusion.94
  150.0 1.3 fusion.94
  152.0 1.3 fusion.94
  154.0 1.3 fusion.94
  156.0 1.3 fusion.94
  157.9 1.3 fusion.94
  159.9 1.3 fusion.94
  161.9 1.3 fusion.94
  163.9 1.3 fusion.94
  165.8 1.3 fusion.94
  167.8 1.3 fusion.94
  169.8 1.3 fusion.94
  171.8 1.3 fusion.94
  173.7 1.3 fusion.94
  175.7 1.3 fusion.94
  177.7 1.3 fusion.94
  179.7 1.3 fusion.94
  181.6 1.3 fusion.94
  183.6 1.3 fusion.94
  185.6 1.3 fusion.94
  187.6 1.3 fusion.94
  189.5 1.3 fusion.94
  191.5 1.3 fusion.94
  193.5 1.3 fusion.94
  195.5 1.3 fusion.94
  197.4 1.3 fusion.94
  199.4 1.3 fusion.94
  205.3 1.3 fusion.94
  208.5 6.8 %all-to-all-start = ((bf16[16,512,64]{1,2,0:T(8,128)(2,1)}), bf16[16,512,64]{1,2,0:T(8,128)(2,1)S(1)}, u32[]{:S(2)}, u32[]{:S(2)}) async-start(bf16[16,512,64]{1,2,0:T(8,128)(2,1)} %broadcast_in_dim.90), calls=%async_computation | async-start | bytes 2097152 | tf_op jit(solution)/shard_map/all_to_all | solution.py:29
  217.3 14.3 %all-to-all-done = bf16[16,512,64]{1,2,0:T(8,128)(2,1)S(1)} async-done(((bf16[16,512,64]{1,2,0:T(8,128)(2,1)}), bf16[16,512,64]{1,2,0:T(8,128)(2,1)S(1)}, u32[]{:S(2)}, u32[]{:S(2)}) %all-to-all-start) | async-done | bytes 1048608 | tf_op jit(solution)/shard_map/all_to_all | solution.py:29
  (314 shorter events, 37.2 us)
Async XLA Ops:
  7.2 84.4 %copy-start = (bf16[1,64,2048]{2,1,0:T(8,128)(2,1)S(1)}, bf16[1,64,2048]{2,1,0:T(8,128)(2,1)}, u32[]{:S(2)}) copy-start(bf16[1,64,2048]{2,1,0:T(8,128)(2,1)} %param.35) | copy-start | bytes 786436
  7.2 133.0 %all-gather.2.cloned.1.call-start = ((), (), s32[]{:S(2)}) async-start(), calls=%async_computation.5 | async-start | bytes 4325376 | tf_op jit(solution)/shard_map/all_gather | solution.py:17
  7.2 2.3 copy-start.1
  9.5 1.3 copy-start.4
  10.8 1.0 copy-start.6
  10.8 1.7 copy-start.13
  11.7 1.6 copy-start.10
  11.8 6.3 %copy-start.3 = (bf16[128,2048]{1,0:T(8,128)(2,1)S(1)}, bf16[128,2048]{1,0:T(8,128)(2,1)}, u32[]{:S(2)}) copy-start(bf16[128,2048]{1,0:T(8,128)(2,1)} %param.29) | copy-start | bytes 1572868
  11.8 6.5 %copy-start.9 = (f32[2048]{0:T(1024)S(1)}, f32[2048]{0:T(1024)}, u32[]{:S(2)}) copy-start(f32[2048]{0:T(1024)} %param.30) | copy-start | bytes 24580
  60.7 30.3 %copy-start.16 = (bf16[1,2048,64]{1,2,0:T(8,128)(2,1)S(1)}, bf16[1,2048,64]{1,2,0:T(8,128)(2,1)}, u32[]{:S(2)}) copy-start(bf16[1,2048,64]{1,2,0:T(8,128)(2,1)} %param.33) | copy-start | bytes 786436
  89.9 1.2 copy-start.2
  91.0 1.0 copy-start.8
  99.4 4.6 %copy-start.11 = (f32[512,1]{0,1:T(1,128)S(1)}, f32[512,1]{0,1:T(1,128)}, u32[]{:S(2)}) copy-start(f32[512,1]{0,1:T(1,128)} %param.26) | copy-start | bytes 6148
  99.4 33.2 %copy-start.7 = (bf16[2048,64]{0,1:T(8,128)(2,1)S(1)}, bf16[2048,64]{0,1:T(8,128)(2,1)}, u32[]{:S(2)}) copy-start(bf16[2048,64]{0,1:T(8,128)(2,1)} %param.21) | copy-start | bytes 786436
  99.4 34.0 %copy-start.14 = (f32[64]{0:T(128)S(1)}, f32[64]{0:T(128)}, u32[]{:S(2)}) copy-start(f32[64]{0:T(128)} %param.24) | copy-start | bytes 772
  99.4 34.1 %all-to-all-start.3 = ((bf16[16,32,1,12,128]{4,1,3,2,0:T(8,128)(2,1)}), bf16[16,32,1,12,128]{4,1,3,2,0:T(8,128)(2,1)}, u32[]{:S(2)}, u32[]{:S(2)}) async-start(bf16[16,32,1,12,128]{4,1,3,2,0:T(8,128)(2,1)} %bitcast.147), calls=%async_computation.3 | async-start | bytes 3145728 | tf_op jit(solution)/shard_map/all_to_all | solution.py:45
  135.8 71.6 %all-to-all-start.4 = ((bf16[32,12,128]{2,1,0:T(8,128)(2,1)}), bf16[32,12,128]{2,1,0:T(8,128)(2,1)S(1)}, u32[]{:S(2)}, u32[]{:S(2)}) async-start(bf16[32,12,128]{2,1,0:T(8,128)(2,1)} %copy.55), calls=%async_computation.4 | async-start | bytes 262144 | tf_op jit(solution)/shard_map/all_to_all | solution.py:182
  144.1 63.2 %copy-start.15 = (f32[64]{0:T(128)S(1)}, f32[64]{0:T(128)}, u32[]{:S(2)}) copy-start(f32[64]{0:T(128)} %param.27) | copy-start | bytes 772
  207.3 8.1 %copy-start.12 = (f32[128,2]{0,1:T(2,128)S(1)}, f32[128,2]{0,1:T(2,128)}, u32[]{:S(2)}) copy-start(f32[128,2]{0,1:T(2,128)} %param.32) | copy-start | bytes 3076
  207.4 24.1 %copy-start.5 = (bf16[1024,128]{1,0:T(8,128)(2,1)S(1)}, bf16[1024,128]{1,0:T(8,128)(2,1)}, u32[]{:S(2)}) copy-start(bf16[1024,128]{1,0:T(8,128)(2,1)} %param.28) | copy-start | bytes 786436
  208.5 23.0 %all-to-all-start = ((bf16[16,512,64]{1,2,0:T(8,128)(2,1)}), bf16[16,512,64]{1,2,0:T(8,128)(2,1)S(1)}, u32[]{:S(2)}, u32[]{:S(2)}) async-start(bf16[16,512,64]{1,2,0:T(8,128)(2,1)} %broadcast_in_dim.90), calls=%async_computation | async-start | bytes 2097152 | tf_op jit(solution)/shard_map/all_to_all | solution.py:29
Sparse Core Ops, SparseCore 0:
  13.4 83.5 all-gather.1
where the time goes:
time: 242 us; the launch traced here: 240 us
  blocking collectives  92 us (38%)
  matrix products  60.2 us (25%)
  local copies, waits for them, and re-layouts  22.6 us (9%)
  other arithmetic  18 us (7%)
  starting transfers between devices  15.8 us (7%)
  between operations  14.4 us (6%)
  waiting for transfers between devices  14.3 us (6%)
    dot_general x32, matrix products, block_step(): jnp.einsum('qhd,khd->hqk', queries, key_block, preferred_element_type=jnp...  40.3 us
    all_to_all x1, blocking collectives, body(): lax.all_to_all(share_part, 'ep', split_axis=0, concat_axis=0, tiled=True)  34.5 us
    all_to_all x1, blocking collectives, from_everyone(): lax.all_to_all(jnp.broadcast_to(value[None], (length, *value.shape)), axi...  28.8 us
    all_gather x1, blocking collectives, body(): all_gates = lax.all_gather(log_cache, 'ep', axis=0, tiled=True)  28.7 us
    all_to_all x1, waiting for transfers between devices, from_everyone(): lax.all_to_all(jnp.broadcast_to(value[None], (length, *value.shape)), axi...  14.3 us
    dot_general x32, matrix products, block_step(): jnp.einsum('hqk,khd->hqd', expo_scores.astype(jnp.bfloat16), value_block,...  11.6 us
    reduce_sum x32, other arithmetic, block_step(): running_sum = running_sum * rescale + jnp.sum(expo_scores, axis=2)  7.68 us
    all_to_all x1, starting transfers between devices, from_everyone(): lax.all_to_all(jnp.broadcast_to(value[None], (length, *value.shape)), axi...  6.82 us
  transfers between devices with their start and end apart: 4, of which 1 were waited for; matrix products, arithmetic and copies ran while one was open for 38% of the time, Pallas kernels for 0%

commit v1 on v0

v1 whole, which is shorter than its diff:
```python
import functools

import jax
import jax.numpy as jnp
from jax import lax
from jax.experimental import pallas as pl
from jax.experimental.pallas import tpu as pltpu
from jax.sharding import PartitionSpec as P

HD = 64
EPS = 1e-06
GR = 16
KR = HD + GR
BR = KR + HD
SIDE = 4
SLOT = 16
MESH = pl.DeviceIdType.MESH
F32 = jnp.float32
BF16 = jnp.bfloat16


def dot(a, b, dims=((1,), (0,))):
    return lax.dot_general(a, b, (dims, ((), ())), preferred_element_type=F32)


def iota(shape, dim):
    return lax.broadcasted_iota(jnp.int32, shape, dim)


def norm_rows(x, gain):
    return x * lax.rsqrt(jnp.mean(x * x, axis=-1, keepdims=True) + EPS) * gain


def to_row(col):
    n = col.shape[0]
    eye = iota((n, n), 0) == iota((n, n), 1)
    return jnp.sum(jnp.where(eye, col, 0.0), axis=0, keepdims=True)


def to_col(row):
    n = row.shape[1]
    eye = iota((n, n), 0) == iota((n, n), 1)
    return jnp.sum(jnp.where(eye, row, 0.0), axis=1, keepdims=True)


def local(src, dst, sem):
    return pltpu.make_async_copy(src, dst, sem)


def send(src, dst, ssem, rsem, ep, tp):
    return pltpu.make_async_remote_copy(
        src_ref=src,
        dst_ref=dst,
        send_sem=ssem,
        recv_sem=rsem,
        device_id=(ep, tp),
        device_id_type=MESH,
    )


class Torus:
    def __init__(self, colour, ep, tp):
        y, x = lax.div(tp, SIDE), lax.rem(tp, SIDE)
        self.ep, self.tp, self.colour = ep, tp, colour
        self.a, self.b = (y, x) if colour == 0 else (x, y)

    def at(self, a, b):
        a, b = lax.rem(a + SIDE, SIDE), lax.rem(b + SIDE, SIDE)
        return a * SIDE + b if self.colour == 0 else b * SIDE + a


class Gather:
    def __init__(self, torus, buf, half, ssem, rsem):
        self.t, self.buf, self.half, self.ss, self.rs = torus, buf, half, ssem, rsem
        a, b = torus.a, torus.b
        self.am, self.ap, self.ao = (lax.rem(a + k, SIDE) for k in (3, 1, 2))
        self.bm, self.bp, self.bo = (lax.rem(b + k, SIDE) for k in (3, 1, 2))
        t, h = torus, half
        buf = self.buf
        lo, hi = pl.ds(0, h), pl.ds(h, h)
        lo2, hi2 = pl.ds(0, SIDE // 2), pl.ds(SIDE // 2, SIDE // 2)
        right_b, left_b = t.at(a, b + 1), t.at(a, b - 1)
        right_a, left_a = t.at(a + 1, b), t.at(a - 1, b)
        self.out = [
            (buf.at[a, b], right_b),
            (buf.at[a, b], left_b),
            (buf.at[a, self.bm, lo], right_b),
            (buf.at[a, self.bp, hi], left_b),
            (buf.at[a], right_a),
            (buf.at[a], left_a),
            (buf.at[self.am, lo2], right_a),
            (buf.at[self.ap, hi2], left_a),
        ]
        self.inn = [
            buf.at[a, self.bm],
            buf.at[a, self.bp],
            buf.at[a, self.bo, lo],
            buf.at[a, self.bo, hi],
            buf.at[self.am],
            buf.at[self.ap],
            buf.at[self.ao, lo2],
            buf.at[self.ao, hi2],
        ]

    def start(self, k):
        src, to = self.out[k]
        send(src, src, self.ss.at[k], self.rs.at[k], self.t.ep, to).start()

    def arrive(self, k):
        dst = self.inn[k]
        send(dst, dst, self.ss.at[k], self.rs.at[k], self.t.ep, self.t.tp).wait_recv()

    def sent(self):
        for k in range(8):
            src, to = self.out[k]
            send(src, src, self.ss.at[k], self.rs.at[k], self.t.ep, to).wait_send()

    def stages(self):
        return [
            lambda: [self.start(0), self.start(1)],
            lambda: [self.arrive(0), self.start(2), self.arrive(1), self.start(3)],
            lambda: [self.arrive(2), self.arrive(3), self.start(4), self.start(5)],
            lambda: [self.arrive(4), self.start(6), self.arrive(5), self.start(7)],
            lambda: [self.arrive(6), self.arrive(7), self.sent()],
        ]


class Reduce:
    def __init__(self, torus, part, ra, rb, sa, sb, own, ssem, rsem):
        self.t, self.part, self.ra, self.rb, self.sa, self.sb, self.own = (
            torus,
            part,
            ra,
            rb,
            sa,
            sb,
            own,
        )
        self.ss, self.rs = ssem, rsem
        a, b = torus.a, torus.b
        self.am, self.ap, self.ao = (lax.rem(a + k, SIDE) for k in (3, 1, 2))
        self.bm, self.bp, self.bo = (lax.rem(b + k, SIDE) for k in (3, 1, 2))
        t = torus
        h = own.shape[1] // 2
        self.h = h
        lo2, hi2 = pl.ds(0, SIDE // 2), pl.ds(SIDE // 2, SIDE // 2)
        lo, hi = pl.ds(0, h), pl.ds(h, h)
        right_b, left_b = t.at(a, b + 1), t.at(a, b - 1)
        right_a, left_a = t.at(a + 1, b), t.at(a - 1, b)
        self.out = [
            (part.at[self.ao, lo2], ra.at[2, lo2], right_a),
            (part.at[self.ao, hi2], ra.at[2, hi2], left_a),
            (sa.at[0], ra.at[0], right_a),
            (sa.at[1], ra.at[1], left_a),
            (own.at[self.bo, lo], rb.at[2, lo], right_b),
            (own.at[self.bo, hi], rb.at[2, hi], left_b),
            (sb.at[0], rb.at[0], right_b),
            (sb.at[1], rb.at[1], left_b),
        ]

    def start(self, k):
        src, dst, to = self.out[k]
        send(src, dst, self.ss.at[k], self.rs.at[k], self.t.ep, to).start()

    def arrive(self, k):
        _, dst, to = self.out[k]
        send(dst, dst, self.ss.at[k], self.rs.at[k], self.t.ep, to).wait_recv()

    def sent(self):
        for k in range(8):
            src, dst, to = self.out[k]
            send(src, dst, self.ss.at[k], self.rs.at[k], self.t.ep, to).wait_send()

    def first(self):
        self.start(0)
        self.start(1)

    def second(self):
        p, ra, sa = self.part, self.ra, self.sa
        half = SIDE // 2
        sa[0, half:] = p[self.ap, half:]
        sa[1, :half] = p[self.am, :half]
        self.arrive(0)
        sa[0, :half] = (p[self.ap, :half].astype(F32) + ra[2, :half].astype(F32)).astype(BF16)
        self.start(2)
        self.arrive(1)
        sa[1, half:] = (p[self.am, half:].astype(F32) + ra[2, half:].astype(F32)).astype(BF16)
        self.start(3)

    def third(self):
        p, ra = self.part, self.ra
        self.arrive(2)
        self.arrive(3)

        def one(j, _):
            self.own[j] = (
                p[self.t.a, j].astype(F32) + ra[0, j].astype(F32) + ra[1, j].astype(F32)
            ).astype(BF16)
            return 0

        lax.fori_loop(0, SIDE, one, 0)
        self.start(4)
        self.start(5)

    def fourth(self):
        o, rb, sb, h = self.own, self.rb, self.sb, self.h
        sb[0, h:] = o[self.bp, h:]
        sb[1, :h] = o[self.bm, :h]
        self.arrive(4)
        sb[0, :h] = (o[self.bp, :h].astype(F32) + rb[2, :h].astype(F32)).astype(BF16)
        self.start(6)
        self.arrive(5)
        sb[1, h:] = (o[self.bm, h:].astype(F32) + rb[2, h:].astype(F32)).astype(BF16)
        self.start(7)

    def result(self):
        self.arrive(6)
        self.arrive(7)
        r = (
            self.own[self.t.b].astype(F32) + self.rb[0].astype(F32) + self.rb[1].astype(F32)
        ).astype(BF16)
        self.sent()
        return r


class Exchange:
    def __init__(self, ep, tp, n, src, dst, ssem, rsem):
        self.ep, self.tp, self.n = ep, tp, n
        self.src, self.dst, self.ss, self.rs = src, dst, ssem, rsem

    def start(self):
        self.dst[self.ep] = self.src[self.ep]

        def one(i, _):
            step = lax.select(lax.rem(i, 2) == 1, lax.div(i + 1, 2), self.n - lax.div(i, 2))
            peer = lax.rem(self.ep + step, self.n)
            send(
                self.src.at[peer],
                self.dst.at[self.ep],
                self.ss.at[peer],
                self.rs.at[self.ep],
                peer,
                self.tp,
            ).start()
            return 0

        lax.fori_loop(1, self.n, one, 0)

    def arrive(self):
        def one(i, _):
            peer = lax.rem(self.ep + i, self.n)
            d = send(
                self.src.at[peer],
                self.dst.at[peer],
                self.ss.at[peer],
                self.rs.at[peer],
                peer,
                self.tp,
            )
            d.wait_recv()
            d.wait_send()
            return 0

        lax.fori_loop(1, self.n, one, 0)


def kernel(
    n_ep,
    n_tp,
    x_h,
    mix_gain,
    wq_h,
    wk_h,
    wv_h,
    q_gain,
    k_gain,
    gates,
    h_gain,
    wo_h,
    mx_h,
    moe_gain,
    routes,
    rweight,
    wg_h,
    wu_h,
    wd_h,
    mixer_out,
    moe_out,
    x,
    nx,
    wq,
    wk,
    wv,
    wo,
    mx,
    wg,
    wu,
    wd,
    kv,
    qa,
    acc,
    mx_run,
    hg0,
    hg1,
    sendb,
    recvb,
    retb,
    backb,
    onehot,
    g0,
    g1,
    part0,
    part1,
    ra0,
    ra1,
    rb0,
    rb1,
    sa0,
    sa1,
    sb0,
    sb1,
    own0,
    own1,
    load_sem,
    kv_recv,
    up_send,
    dn_send,
    sib_send,
    hg_s,
    hg_r,
    mg_s,
    mg_r,
    rd_s,
    rd_r,
    d_s,
    d_r,
    b_s,
    b_r,
):
    ep, tp = lax.axis_index("ep"), lax.axis_index("tp")
    z, core = lax.div(ep, 2), lax.rem(ep, 2)
    nz = n_ep // 2
    ups, dns = nz // 2, nz - 1 - nz // 2
    tq = x.shape[0]
    half_t = tq // 2

    loads = [
        local(s, d, load_sem.at[i])
        for i, (s, d) in enumerate(
            [
                (mx_h, mx),
                (x_h, x),
                (wq_h, wq),
                (wk_h, wk),
                (wv_h, wv),
                (wg_h.at[0], wg),
                (wu_h.at[0], wu),
                (wd_h.at[0], wd),
                (wo_h, wo),
            ]
        )
    ]
    for d in loads:
        d.start()

    barrier = pltpu.get_barrier_semaphore()

    def greet_ep(i, _):
        pl.semaphore_signal(
            barrier, inc=1, device_id=(lax.rem(ep + i, n_ep), tp), device_id_type=MESH
        )
        return 0

    def greet_tp(i, _):
        pl.semaphore_signal(
            barrier, inc=1, device_id=(ep, lax.rem(tp + i, n_tp)), device_id_type=MESH
        )
        return 0

    lax.fori_loop(1, n_ep, greet_ep, 0)
    lax.fori_loop(1, n_tp, greet_tp, 0)

    toks = mx.shape[0]
    slots = n_ep * SLOT
    loads[0].wait()
    r_col = routes[...].astype(F32)
    r_rows = [to_row(r_col[:, k : k + 1]) for k in range(2)]
    experts = iota((n_ep, toks), 0).astype(F32)
    hot = [(experts == r).astype(F32) for r in r_rows]
    before = (iota((toks, toks), 0) < iota((toks, toks), 1)).astype(BF16)
    counts = dot((hot[0] + hot[1]).astype(BF16), before)
    for k in range(2):
        order = jnp.sum(hot[k] * counts, axis=0, keepdims=True)
        slot = (r_rows[k] * SLOT + order).astype(jnp.int32)
        onehot[k] = (iota((slots, toks), 0) == slot).astype(F32).astype(BF16)
    mxf = mx[...].astype(F32)
    mscale = lax.rsqrt(jnp.mean(mxf * mxf, axis=-1, keepdims=True) + EPS)
    cols = pl.ds(pl.multiple_of(tp * 128, 128), 128)
    mslice = (mx[:, cols].astype(F32) * mscale * moe_gain[:, cols]).astype(BF16)
    both = (onehot[0].astype(F32) + onehot[1].astype(F32)).astype(BF16)
    sendb[...] = dot(both, mslice).astype(BF16).reshape(n_ep, SLOT, 128)

    loads[1].wait()

    def norm_some(i, _):
        rows = pl.ds(pl.multiple_of(i * 64, 64), 64)
        nx[rows, :] = norm_rows(x[rows, :].astype(F32), mix_gain[...]).astype(BF16)
        return 0

    lax.fori_loop(0, tq // 64, norm_some, 0)
    for d in loads[2:5]:
        d.wait()
    n_all = nx[...]
    q = norm_rows(dot(n_all, wq[...]), q_gain[...]) * (HD**-0.5)
    k = norm_rows(dot(n_all, wk[...]), k_gain[...])
    v = dot(n_all, wv[...])
    qa[0:HD, :] = q.T.astype(BF16)
    ridx = iota((GR, tq), 0)
    qa[HD:KR, :] = jnp.where(ridx < 3, -1.0, 0.0).astype(BF16)
    g = gates[...]
    ghi = g.astype(BF16).astype(F32)
    gmid = (g - ghi).astype(BF16).astype(F32)
    glo = g - ghi - gmid
    grow = jnp.where(
        ridx == 0,
        ghi,
        jnp.where(ridx == 1, gmid, jnp.where(ridx == 2, glo, jnp.where(ridx == 3, 1.0, 0.0))),
    ).astype(BF16)
    kt, vt = k.T.astype(BF16), v.T.astype(BF16)
    for c in range(2):
        cc = slice(c * half_t, (c + 1) * half_t)
        kv[ep, c, 0:HD, :] = kt[:, cc]
        kv[ep, c, HD:KR, :] = grow[:, cc]
        kv[ep, c, KR:BR, :] = vt[:, cc]

    pl.semaphore_wait(barrier, n_ep - 1 + n_tp - 1)

    dispatch = Exchange(ep, tp, n_ep, sendb, recvb, d_s, d_r)
    dispatch.start()

    def hop(slot, c, to_ep, ssem):
        return send(kv.at[slot, c], kv.at[slot, c], ssem, kv_recv.at[slot, c], to_ep, tp)

    up_ep = lax.rem(z + 1, nz) * 2 + core
    dn_ep = lax.rem(z + nz - 1, nz) * 2 + core
    sib_ep = z * 2 + 1 - core

    def slot_of(step, whose):
        return lax.rem(z + step + nz, nz) * 2 + whose

    for c in range(2):
        hop(ep, c, up_ep, up_send.at[0, c]).start()
        hop(ep, c, dn_ep, dn_send.at[0, c]).start()
        hop(ep, c, sib_ep, sib_send.at[ep, c]).start()

    def flash(slot, diagonal=False):
        s = [dot(kv[slot, c, 0:KR, :], qa[...], ((0,), (0,))) for c in range(2)]
        if diagonal:
            s = [
                jnp.where(
                    iota((half_t, tq), 0) + c * half_t <= iota((half_t, tq), 1), s[c], -1e30
                )
                for c in range(2)
            ]
        top = jnp.maximum(
            jnp.max(s[0], axis=0, keepdims=True), jnp.max(s[1], axis=0, keepdims=True)
        )
        if diagonal:
            new = top
        else:
            old = mx_run[...]
            new = jnp.maximum(old, top)
        got = None
        for c in range(2):
            w = jnp.exp(s[c] - new).astype(BF16)
            o = dot(kv[slot, c, HD:BR, :], w)
            got = o if got is None else got + o
        if diagonal:
            acc[...] = got
        else:
            acc[...] = acc[...] * jnp.exp(old - new) + got
        mx_run[...] = new

    flash(ep, diagonal=True)

    def take(slot):
        @pl.when(slot < ep)
        def _():
            flash(slot)

    def wait_block(slot, c):
        hop(slot, c, sib_ep, sib_send.at[slot, c]).wait_recv()

    t0, t1 = Torus(0, ep, tp), Torus(1, ep, tp)
    rows = g0.shape[2]
    mg = [
        Gather(t0, g0, rows // 2, mg_s.at[0], mg_r.at[0]),
        Gather(t1, g1, rows // 2, mg_s.at[1], mg_r.at[1]),
    ]
    rd = [
        Reduce(t0, part0, ra0, rb0, sa0, sb0, own0, rd_s.at[0], rd_r.at[0]),
        Reduce(t1, part1, ra1, rb1, sa1, sb1, own1, rd_s.at[1], rd_r.at[1]),
    ]
    cap = 2 * rows // n_ep
    returns = Exchange(ep, tp, n_ep, retb, backb, b_s, b_r)

    def pick(rows_out, rows_in, wide_first):
        wide, dense = (0, 1) if wide_first else (1, 0)
        w, d = iota((rows_out, rows_in), wide), iota((rows_out, rows_in), dense)
        i = lax.rem(w, SLOT)
        hit = jnp.logical_and(lax.div(w, SLOT) * cap + i == d, i < cap)
        return hit.astype(F32).astype(BF16)

    def pack_rows():
        dispatch.arrive()
        packed = dot(
            pick(2 * rows, slots, False), recvb[...].reshape(slots, 128)
        ).astype(BF16)
        g0[t0.a, t0.b] = packed[:rows]
        g1[t1.a, t1.b] = packed[rows:]
        for m in mg:
            m.stages()[0]()

    def experts_now():
        for d in loads[5:8]:
            d.wait()
        for m, buf, part in ((mg[0], g0, part0), (mg[1], g1, part1)):
            m.stages()[4]()
            gs = us = None
            for a in range(SIDE):
                for b in range(SIDE):
                    t = a * SIDE + b if m.t.colour == 0 else b * SIDE + a
                    blk = buf[a, b]
                    p = dot(blk, wg[t * 128 : (t + 1) * 128, :])
                    r = dot(blk, wu[t * 128 : (t + 1) * 128, :])
                    gs = p if gs is None else gs + p
                    us = r if us is None else us + r
            hidden = (gs / (1.0 + jnp.exp(-gs)) * us).astype(BF16)
            for a in range(SIDE):
                for b in range(SIDE):
                    t = a * SIDE + b if m.t.colour == 0 else b * SIDE + a
                    part[a, b] = dot(hidden, wd[:, t * 128 : (t + 1) * 128]).astype(BF16)
        for r in rd:
            r.first()

    def give_back():
        summed = jnp.concatenate([rd[0].result(), rd[1].result()], axis=0)
        retb[...] = (
            dot(pick(slots, 2 * rows, True), summed).astype(BF16).reshape(n_ep, SLOT, 128)
        )
        returns.start()

    hooks = {
        3: pack_rows,
        4: lambda: [m.stages()[1]() for m in mg],
        5: lambda: [m.stages()[2]() for m in mg],
        6: lambda: [m.stages()[3]() for m in mg],
        8: experts_now,
    }

    def ring(s, _):
        up, dn = slot_of(-s, core), slot_of(s, core)
        for c in range(2):
            wait_block(up, c)

            @pl.when(s < ups)
            def _():
                hop(up, c, up_ep, up_send.at[s, c]).start()

            hop(up, c, sib_ep, sib_send.at[up, c]).start()

            @pl.when(s <= dns)
            def _():
                wait_block(dn, c)

                @pl.when(s < dns)
                def _():
                    hop(dn, c, dn_ep, dn_send.at[s, c]).start()

                hop(dn, c, sib_ep, sib_send.at[dn, c]).start()

            if c == 0:
                def handed(i, _):
                    far = slot_of(lax.select(i == 0, 1 - s, s - 1), 1 - core)

                    @pl.when(jnp.logical_or(i == 0, s >= 2))
                    def _():
                        wait_block(far, 0)
                        wait_block(far, 1)
                        take(far)

                    return 0

                lax.fori_loop(0, 2, handed, 0)

        def came(i, _):
            near = slot_of(lax.select(i == 0, -s, s), core)

            @pl.when(jnp.logical_or(i == 0, s <= dns))
            def _():
                take(near)

            return 0

        lax.fori_loop(0, 2, came, 0)
        for at, hook in hooks.items():

            @pl.when(s == at)
            def _():
                hook()

        return 0

    lax.fori_loop(1, ups + 1, ring, 0)
    last = slot_of(-ups, 1 - core)
    wait_block(last, 0)
    wait_block(last, 1)
    take(last)

    for r in rd:
        r.second()
    att = acc[GR:, :] / acc[3:4, :]
    att = att * lax.rsqrt(jnp.mean(att * att, axis=0, keepdims=True) + EPS)
    head = (att * to_col(h_gain[...])).astype(BF16)
    hg0[t0.a, t0.b] = head[:, :half_t]
    hg1[t1.a, t1.b] = head[:, half_t:]
    hg = [
        Gather(t0, hg0, HD // 2, hg_s.at[0], hg_r.at[0]),
        Gather(t1, hg1, HD // 2, hg_s.at[1], hg_r.at[1]),
    ]
    for m in hg:
        m.stages()[0]()
    for r in rd:
        r.third()
    for m in hg:
        m.stages()[1]()
    for r in rd:
        r.fourth()
    for m in hg:
        m.stages()[2]()
    give_back()
    for m in hg:
        m.stages()[3]()
    loads[8].wait()
    for i, (m, buf) in enumerate(((hg[0], hg0), (hg[1], hg1))):
        m.stages()[4]()
        o = None
        for a in range(SIDE):
            for b in range(SIDE):
                t = a * SIDE + b if i == 0 else b * SIDE + a
                p = dot(buf[a, b], wo[t * HD : (t + 1) * HD, :], ((0,), (0,)))
                o = p if o is None else o + p
        mixer_out[i * half_t : (i + 1) * half_t, :] = o.astype(BF16)

    returns.arrive()
    back = backb[...].reshape(slots, 128)
    total = None
    for k in range(2):
        got = dot(onehot[k], back, ((0,), (0,))) * rweight[:, k : k + 1]
        total = got if total is None else total + got
    moe_out[...] = total.astype(BF16)

    def up_done(s, _):
        for c in range(2):
            hop(slot_of(-s, core), c, up_ep, up_send.at[s, c]).wait_send()
        return 0

    def dn_done(s, _):
        for c in range(2):
            hop(slot_of(s, core), c, dn_ep, dn_send.at[s, c]).wait_send()
        return 0

    def sib_done(i, _):
        for c in range(2):
            slot = i * 2 + core
            hop(slot, c, sib_ep, sib_send.at[slot, c]).wait_send()
        return 0

    lax.fori_loop(0, ups, up_done, 0)
    lax.fori_loop(0, dns, dn_done, 0)
    lax.fori_loop(0, nz, sib_done, 0)


def body(
    n_ep,
    n_tp,
    attn_in,
    mix_gain,
    query_weight,
    key_weight,
    value_weight,
    query_gain,
    key_gain,
    log_cache,
    head_gain,
    out_weight,
    moe_in,
    moe_gain,
    routes,
    route_weight,
    expert_gate,
    expert_up,
    expert_down,
):
    tq, d = attn_in.shape
    toks = moe_in.shape[0]
    cap = 3 * toks * routes.shape[1] // (2 * n_ep)
    rows = n_ep * cap // 2
    vm = pl.BlockSpec(memory_space=pltpu.VMEM)
    hbm = pl.BlockSpec(memory_space=pl.ANY)
    dma = pltpu.SemaphoreType.DMA

    def v(*shape, dtype=BF16):
        return pltpu.VMEM(shape, dtype)

    nz = n_ep // 2
    scratch = [
        v(tq, d),
        v(tq, d),
        v(d, HD),
        v(d, HD),
        v(d, HD),
        v(n_tp * HD, 128),
        v(toks, d),
        v(d, 64),
        v(d, 64),
        v(64, d),
        v(n_ep, 2, BR, tq // 2),
        v(KR, tq),
        v(GR + HD, tq, dtype=F32),
        v(1, tq, dtype=F32),
        v(SIDE, SIDE, HD, tq // 2),
        v(SIDE, SIDE, HD, tq // 2),
        v(n_ep, SLOT, 128),
        v(n_ep, SLOT, 128),
        v(n_ep, SLOT, 128),
        v(n_ep, SLOT, 128),
        v(2, n_ep * SLOT, toks),
        v(SIDE, SIDE, rows, 128),
        v(SIDE, SIDE, rows, 128),
        v(SIDE, SIDE, rows, 128),
        v(SIDE, SIDE, rows, 128),
        v(3, SIDE, rows, 128),
        v(3, SIDE, rows, 128),
        v(3, rows, 128),
        v(3, rows, 128),
        v(2, SIDE, rows, 128),
        v(2, SIDE, rows, 128),
        v(2, rows, 128),
        v(2, rows, 128),
        v(SIDE, rows, 128),
        v(SIDE, rows, 128),
        dma((9,)),
        dma((n_ep, 2)),
        dma((nz, 2)),
        dma((nz, 2)),
        dma((n_ep, 2)),
        dma((2, 8)),
        dma((2, 8)),
        dma((2, 8)),
        dma((2, 8)),
        dma((2, 8)),
        dma((2, 8)),
        dma((n_ep,)),
        dma((n_ep,)),
        dma((n_ep,)),
        dma((n_ep,)),
    ]
    return pl.pallas_call(
        functools.partial(kernel, n_ep, n_tp),
        out_shape=(
            jax.ShapeDtypeStruct((tq, 128), BF16),
            jax.ShapeDtypeStruct((toks, 128), BF16),
        ),
        in_specs=[hbm, vm, hbm, hbm, hbm, vm, vm, vm, vm, hbm, hbm, vm, vm, vm, hbm, hbm, hbm],
        out_specs=(vm, vm),
        scratch_shapes=scratch,
        compiler_params=pltpu.CompilerParams(
            collective_id=0, has_side_effects=True, vmem_limit_bytes=60 * 1024 * 1024
        ),
    )(
        attn_in,
        mix_gain.reshape(1, -1),
        query_weight,
        key_weight,
        value_weight,
        query_gain.reshape(1, -1),
        key_gain.reshape(1, -1),
        log_cache.reshape(1, -1),
        head_gain.reshape(1, -1),
        out_weight,
        moe_in,
        moe_gain.reshape(1, -1),
        routes,
        route_weight,
        expert_gate,
        expert_up,
        expert_down,
    )


def solution(mesh):
    n_ep, n_tp = mesh.shape["ep"], mesh.shape["tp"]
    in_specs = (
        P("ep", None),
        P(),
        P(None, "tp"),
        P(None, "tp"),
        P(None, "tp"),
        P(),
        P(),
        P("ep", "tp"),
        P("tp"),
        P(None, "tp"),
        P("ep", None),
        P(),
        P("ep", None),
        P("ep", None),
        P("ep", None, "tp"),
        P("ep", None, "tp"),
        P("ep", "tp", None),
    )
    out_specs = (P("ep", "tp"), P("ep", "tp"))
    return jax.shard_map(
        functools.partial(body, n_ep, n_tp),
        mesh=mesh,
        in_specs=in_specs,
        out_specs=out_specs,
        check_vma=False,
    )
```

time: 242 us -> 107 us (0.44)
  Pallas kernels: 0 us -> 92.5 us
  blocking collectives: 92 us -> 0 us
  matrix products: 60.2 us -> 0 us
  other arithmetic: 18 us -> 0 us
  starting transfers between devices: 15.8 us -> 0 us
  waiting for transfers between devices: 14.3 us -> 0 us
  between operations: 14.4 us -> 0.66 us
  local copies, waits for them, and re-layouts: 22.6 us -> 13.7 us
    pallas_call x0 -> x1, Pallas kernels: none -> 92.5 us  [body(): pl.pallas_call(functools.partial(kernel, n_ep, n_tp), out_shape=(jax.Shap...]
    all_to_all x2 -> x0, blocking collectives: 63.3 us -> none  [the longest x1 34.5 us: body(): lax.all_to_all(share_part, 'ep', split_axis=0, concat_axis=0, tiled=True)]
    dot_general x70 -> x0, matrix products: 60.2 us -> none  [the longest x32 40.3 us: block_step(): jnp.einsum('qhd,khd->hqk', queries, key_block, preferred_element_type=jnp...]
    all_gather x1 -> x0, blocking collectives: 28.7 us -> none  [body(): all_gates = lax.all_gather(log_cache, 'ep', axis=0, tiled=True)]
    all_to_all x3 -> x0, starting transfers between devices: 15.7 us -> none  [the longest x1 6.82 us: from_everyone(): lax.all_to_all(jnp.broadcast_to(value[None], (length, *value.shape)), axi...]
    all_to_all x3 -> x0, waiting for transfers between devices: 14.3 us -> none  [the longest x1 14.3 us: from_everyone(): lax.all_to_all(jnp.broadcast_to(value[None], (length, *value.shape)), axi...]
    reduce_sum x38 -> x0, other arithmetic: 12.7 us -> none  [the longest x32 7.68 us: block_step(): running_sum = running_sum * rescale + jnp.sum(expo_scores, axis=2)]
    unnamed x36 -> x13, local copies, waits for them, and re-layouts: 2.03 us -> 13.7 us
  transfers between devices with their start and end apart: 4 -> 0, of which waited for: 1 -> 0; matrix products, arithmetic and copies ran while one was open for 38% -> 0% of each run, Pallas kernels for 0% -> 0%
where the time goes in v1:
time: 107 us
  Pallas kernels  92.5 us (86%)
  local copies, waits for them, and re-layouts  13.7 us (13%)
    pallas_call x1, Pallas kernels, body(): pl.pallas_call(functools.partial(kernel, n_ep, n_tp), out_shape=(jax.Shap...  92.5 us
    unnamed x13, local copies, waits for them, and re-layouts  13.7 us

profile of v1, /device:TPU:1, one launch (start us, length us, event | category | flops | bytes accessed | tf_op | source)
XLA Modules:
  0.0 106.9 jit_solution(7369342286512959863)
XLA Ops:
  0.6 0.0 copy-start.1
  0.6 0.0 copy-start
  0.7 1.5 %copy.22.routes = s32[128,2]{1,0:T(8,128)} copy(s32[128,2]{0,1:T(2,128)} %param.29) | data formatting | bytes 2048 | tf_op args[12]
  2.1 1.4 %copy.23.rweight = f32[128,2]{1,0:T(8,128)} copy(f32[128,2]{0,1:T(2,128)} %param.30) | data formatting | bytes 2048 | tf_op args[13]
  3.5 2.0 %copy.19.wq_h = bf16[2048,64]{1,0:T(8,128)(2,1)} copy(bf16[2048,64]{0,1:T(8,128)(2,1)} %param.19) | data formatting | bytes 524288 | tf_op args[2]
  5.5 2.0 %copy.20.wk_h = bf16[2048,64]{1,0:T(8,128)(2,1)} copy(bf16[2048,64]{0,1:T(8,128)(2,1)} %param.20) | data formatting | bytes 524288 | tf_op args[3]
  7.4 2.0 %copy.21.wv_h = bf16[2048,64]{1,0:T(8,128)(2,1)} copy(bf16[2048,64]{0,1:T(8,128)(2,1)} %param.21) | data formatting | bytes 524288 | tf_op args[4]
  9.4 0.0 copy-done
  9.4 1.0 copy.24.wg_h
  10.4 0.0 copy-done.1
  10.4 1.0 copy.25.wu_h
  11.4 92.5 %shard_map.176 = (bf16[512,128]{1,0:T(8,128)(2,1)}, bf16[128,128]{1,0:T(8,128)(2,1)}) custom-call(bf16[512,2048]{1,0:T(8,128)(2,1)} %x_h.1, f32[1,2048]{1,0:T(1,128)} %bitcast.6, bf16[2048,64]{1,0:T(8,128)(2,1)} %copy.19.wq_h, bf16[2048,64]{1,0:T(8,128)(2,1)} %copy.20.wk_h, bf16[2048,64]{1,0:T(8,128)(2,1)} %copy.21.wv_h, f32[1,64]{1,0:T(1,128)} %bitcast.9, ...), custom_call_target="tpu_custom_call" | custom-call | tf_op jit(solution)/shard_map/pallas_call | solution.py:769
  104.0 1.6 %copy.28 = bf16[512,128]{1,0:T(8,128)(2,1)} copy(bf16[512,128]{1,0:T(8,128)(2,1)} %get-tuple-element.4) | data formatting | bytes 262144
  105.5 1.4 %copy.29 = bf16[128,128]{1,0:T(8,128)(2,1)} copy(bf16[128,128]{1,0:T(8,128)(2,1)} %get-tuple-element.5) | data formatting | bytes 65536
Async XLA Ops:
  0.6 9.8 %copy-start.1 = (bf16[1,2048,64]{1,2,0:T(8,128)(2,1)S(1)}, bf16[1,2048,64]{1,2,0:T(8,128)(2,1)}, u32[]{:S(2)}) copy-start(bf16[1,2048,64]{1,2,0:T(8,128)(2,1)} %param.32) | copy-start | bytes 786436
  0.6 8.8 %copy-start = (bf16[1,2048,64]{1,2,0:T(8,128)(2,1)S(1)}, bf16[1,2048,64]{1,2,0:T(8,128)(2,1)}, u32[]{:S(2)}) copy-start(bf16[1,2048,64]{1,2,0:T(8,128)(2,1)} %param.31) | copy-start | bytes 786436

commit v2 on v1

v2 whole, which is shorter than its diff:
```python
import functools

import jax
import jax.numpy as jnp
from jax import lax
from jax.experimental import pallas as pl
from jax.experimental.pallas import tpu as pltpu
from jax.sharding import PartitionSpec as P

HD = 64
EPS = 1e-06
GR = 8
KR = HD + GR
BR = KR + HD
SIDE = 4
SLOT = 16
NCH = 4
NH = NCH // 2
MESH = pl.DeviceIdType.MESH
F32 = jnp.float32
BF16 = jnp.bfloat16


def dot(a, b, dims=((1,), (0,))):
    return lax.dot_general(a, b, (dims, ((), ())), preferred_element_type=F32)


def iota(shape, dim):
    return lax.broadcasted_iota(jnp.int32, shape, dim)


def norm_rows(x, gain):
    return x * lax.rsqrt(jnp.mean(x * x, axis=-1, keepdims=True) + EPS) * gain


def norm_cols(x, gain):
    return x * lax.rsqrt(jnp.mean(x * x, axis=0, keepdims=True) + EPS) * gain


def to_col(row):
    n = row.shape[1]
    eye = iota((n, n), 0) == iota((n, n), 1)
    return jnp.sum(jnp.where(eye, row, 0.0), axis=1, keepdims=True)


def local(src, dst, sem):
    return pltpu.make_async_copy(src, dst, sem)


def send(src, dst, ssem, rsem, ep, tp):
    return pltpu.make_async_remote_copy(
        src_ref=src,
        dst_ref=dst,
        send_sem=ssem,
        recv_sem=rsem,
        device_id=(ep, tp),
        device_id_type=MESH,
    )


class Torus:
    def __init__(self, colour, ep, tp):
        y, x = lax.div(tp, SIDE), lax.rem(tp, SIDE)
        self.ep, self.tp, self.colour = ep, tp, colour
        self.a, self.b = (y, x) if colour == 0 else (x, y)

    def at(self, a, b):
        a, b = lax.rem(a + SIDE, SIDE), lax.rem(b + SIDE, SIDE)
        return a * SIDE + b if self.colour == 0 else b * SIDE + a


class Gather:
    def __init__(self, torus, buf, half, ssem, rsem):
        self.t, self.buf, self.ss, self.rs = torus, buf, ssem, rsem
        a, b = torus.a, torus.b
        self.am, self.ap = (lax.rem(a + k, SIDE) for k in (3, 1))
        self.bm, self.bp, self.bo = (lax.rem(b + k, SIDE) for k in (3, 1, 2))
        self.lo, self.hi = pl.ds(0, half), pl.ds(half, half)
        self.right_b, self.left_b = torus.at(a, b + 1), torus.at(a, b - 1)
        self.right_a, self.left_a = torus.at(a + 1, b), torus.at(a - 1, b)

    def put(self, block):
        self.buf[SIDE * self.t.a + self.t.b] = block

    def go(self, a, b, to, k, rows=slice(None)):
        src = self.buf.at[SIDE * a + b, rows]
        send(src, src, self.ss, self.rs.at[k], self.t.ep, to).start()

    def whole(self, n, k):
        d = self.buf.at[pl.ds(0, n)]
        return send(d, d, self.ss, self.rs.at[k], self.t.ep, self.t.tp)

    def got(self, k, n):
        self.whole(n, k).wait_recv()

    def stage(self, k):
        a, b = self.t.a, self.t.b
        if k == 0:
            self.go(a, b, self.right_b, 0)
            self.go(a, b, self.left_b, 0)
            self.go(a, b, self.right_a, 2)
            self.go(a, b, self.left_a, 2)
        elif k == 1:
            self.got(0, 2)
            self.go(a, self.bm, self.right_b, 1, self.lo)
            self.go(a, self.bp, self.left_b, 1, self.hi)
            for j in (self.bm, self.bp):
                self.go(a, j, self.right_a, 3)
                self.go(a, j, self.left_a, 3)
        elif k == 2:
            self.got(1, 1)
            self.go(a, self.bo, self.right_a, 4)
            self.go(a, self.bo, self.left_a, 4)
            self.got(2, 2)
            self.go(self.am, b, self.right_a, 5)
            self.got(3, 4)
            self.go(self.am, self.bm, self.right_a, 5)
            self.go(self.ap, self.bp, self.left_a, 5)
        elif k == 3:
            self.got(4, 2)
            self.go(self.ap, self.bo, self.left_a, 5)
        else:
            self.got(5, 4)
            self.whole(SIDE * SIDE - 1, 5).wait_send()


class Exchange:
    def __init__(self, ep, tp, n, cap, src, dst, ssem, rsem):
        self.ep, self.tp, self.n = ep, tp, n
        self.used = pl.ds(0, cap)
        self.src, self.dst, self.ss, self.rs = src, dst, ssem, rsem

    def start(self):
        self.dst[self.ep] = self.src[self.ep]

        def one(i, _):
            step = lax.select(lax.rem(i, 2) == 1, lax.div(i + 1, 2), self.n - lax.div(i, 2))
            peer = lax.rem(self.ep + step, self.n)
            send(
                self.src.at[peer, self.used],
                self.dst.at[self.ep, self.used],
                self.ss,
                self.rs,
                peer,
                self.tp,
            ).start()
            return 0

        lax.fori_loop(1, self.n, one, 0)

    def arrive(self):
        others = pl.ds(0, self.n - 1)
        d = send(
            self.src.at[others, self.used],
            self.dst.at[others, self.used],
            self.ss,
            self.rs,
            self.ep,
            self.tp,
        )
        d.wait_recv()
        d.wait_send()


def kernel(
    n_ep,
    n_tp,
    x_h,
    mix_gain_h,
    wq_h,
    wk_h,
    wv_h,
    q_gain_h,
    k_gain_h,
    gates_h,
    h_gain_h,
    wo_h,
    mx_h,
    moe_gain_h,
    routes_h,
    rweight_h,
    wg_h,
    wu_h,
    wd_h,
    mixer_out,
    moe_out,
    x,
    nx,
    wqkv,
    wo,
    mx,
    wgu,
    wd,
    kv,
    qa,
    acc,
    mx_run,
    hg0,
    hg1,
    sendb,
    recvb,
    retb,
    backb,
    onehot,
    g0,
    g1,
    h0,
    h1,
    wdn,
    mix_gain,
    q_gain,
    k_gain,
    gates,
    h_gain,
    moe_gain,
    routes,
    rweight,
    load_sem,
    near_recv,
    far_recv,
    kv_send,
    hg_s,
    hg_r,
    mg_s,
    mg_r,
    mh_s,
    mh_r,
    wd_s,
    wd_r,
    d_s,
    d_r,
    b_s,
    b_r,
):
    ep, tp = lax.axis_index("ep"), lax.axis_index("tp")
    z, core = lax.div(ep, 2), lax.rem(ep, 2)
    nz = n_ep // 2
    ups, dns = nz // 2, nz - 1 - nz // 2
    tq = x.shape[0]
    half_t = tq // 2
    fh = wd.shape[0]
    cap = 2 * g0.shape[1] // n_ep

    recvb[...] = jnp.zeros_like(recvb)
    backb[...] = jnp.zeros_like(backb)
    barrier = pltpu.get_barrier_semaphore()

    def greet_ep(i, _):
        pl.semaphore_signal(
            barrier, inc=1, device_id=(lax.rem(ep + i, n_ep), tp), device_id_type=MESH
        )
        return 0

    def greet_tp(i, _):
        pl.semaphore_signal(
            barrier, inc=1, device_id=(ep, lax.rem(tp + i, n_tp)), device_id_type=MESH
        )
        return 0

    lax.fori_loop(1, n_ep, greet_ep, 0)
    lax.fori_loop(1, n_tp, greet_tp, 0)

    loads = [
        local(s, d, load_sem.at[i])
        for i, (s, d) in enumerate(
            [
                (mx_h, mx),
                (moe_gain_h, moe_gain),
                (routes_h, routes),
                (x_h, x),
                (mix_gain_h, mix_gain),
                (wq_h, wqkv.at[pl.ds(0, HD)]),
                (wk_h, wqkv.at[pl.ds(HD, HD)]),
                (wv_h, wqkv.at[pl.ds(2 * HD, HD)]),
                (q_gain_h, q_gain),
                (k_gain_h, k_gain),
                (gates_h, gates),
                (wg_h.at[0], wgu.at[pl.ds(0, fh)]),
                (wu_h.at[0], wgu.at[pl.ds(fh, fh)]),
                (wd_h.at[0], wd),
                (wo_h, wo),
                (h_gain_h, h_gain),
                (rweight_h, rweight),
            ]
        )
    ]
    for d in loads:
        d.start()

    toks = mx.shape[0]
    slots = n_ep * SLOT
    for d in loads[0:3]:
        d.wait()
    r_rows = [routes[k : k + 1, :].astype(F32) for k in range(2)]
    experts = iota((n_ep, toks), 0).astype(F32)
    hot = [(experts == r).astype(F32) for r in r_rows]
    before = (iota((toks, toks), 0) < iota((toks, toks), 1)).astype(BF16)
    counts = dot((hot[0] + hot[1]).astype(BF16), before)
    for k in range(2):
        order = jnp.sum(hot[k] * counts, axis=0, keepdims=True)
        slot = (r_rows[k] * SLOT + order).astype(jnp.int32)
        onehot[k] = (iota((slots, toks), 0) == slot).astype(F32).astype(BF16)
    mxf = mx[...].astype(F32)
    mscale = lax.rsqrt(jnp.mean(mxf * mxf, axis=-1, keepdims=True) + EPS)
    cols = pl.ds(pl.multiple_of(tp * 128, 128), 128)
    mslice = (mx[:, cols].astype(F32) * mscale * moe_gain[:, cols]).astype(BF16)
    both = (onehot[0].astype(F32) + onehot[1].astype(F32)).astype(BF16)
    sendb[...] = dot(both, mslice).astype(BF16).reshape(n_ep, SLOT, 128)

    for d in loads[3:5]:
        d.wait()

    def norm_some(i, _):
        rows = pl.ds(pl.multiple_of(i * 64, 64), 64)
        nx[rows, :] = norm_rows(x[rows, :].astype(F32), mix_gain[...]).astype(BF16)
        return 0

    lax.fori_loop(0, tq // 64, norm_some, 0)
    for d in loads[5:11]:
        d.wait()
    qkv = dot(wqkv[...], nx[...], ((1,), (1,)))
    q = norm_cols(qkv[0:HD], to_col(q_gain[...])) * (HD**-0.5)
    k = norm_cols(qkv[HD : 2 * HD], to_col(k_gain[...]))
    qa[0:HD, :] = q.astype(BF16)
    ridx = iota((GR, tq), 0)
    qa[HD:KR, :] = jnp.where(ridx < 3, -1.0, 0.0).astype(BF16)
    g = gates[...]
    ghi = g.astype(BF16).astype(F32)
    gmid = (g - ghi).astype(BF16).astype(F32)
    glo = g - ghi - gmid
    grow = jnp.where(
        ridx == 0,
        ghi,
        jnp.where(ridx == 1, gmid, jnp.where(ridx == 2, glo, jnp.where(ridx == 3, 1.0, 0.0))),
    ).astype(BF16)
    kt, vt = k.astype(BF16), qkv[2 * HD :].astype(BF16)
    piece = tq // NCH
    for c in range(NCH):
        cc = slice(c * piece, (c + 1) * piece)
        kv[ep, c, 0:HD, :] = kt[:, cc]
        kv[ep, c, HD:KR, :] = grow[:, cc]
        kv[ep, c, KR:BR, :] = vt[:, cc]

    pl.semaphore_wait(barrier, n_ep - 1 + n_tp - 1)

    dispatch = Exchange(ep, tp, n_ep, cap, sendb, recvb, d_s, d_r)
    dispatch.start()

    def features(t):
        return wd.at[:, pl.ds(pl.multiple_of(t * 128, 128), 128)]

    def give_weights(i, _):
        peer = lax.rem(tp + i, n_tp)
        send(features(peer), wdn.at[tp], wd_s, wd_r, ep, peer).start()
        return 0

    def take_weights():
        others = wdn.at[pl.ds(0, n_tp - 1)]
        w = send(others, others, wd_s, wd_r, ep, tp)
        w.wait_recv()
        w.wait_send()

    def hop(slot, c, to_ep):
        piece_ref, sem = kv.at[slot, c], near_recv.at[lax.div(slot, 2), c]
        return send(piece_ref, piece_ref, kv_send, sem, to_ep, tp)

    def hand(slot, c):
        piece_ref, sem = kv.at[slot, c], far_recv.at[lax.div(slot, 2)]
        return send(piece_ref, piece_ref, kv_send, sem, sib_ep, tp)

    up_ep = lax.rem(z + 1, nz) * 2 + core
    dn_ep = lax.rem(z + nz - 1, nz) * 2 + core
    sib_ep = z * 2 + 1 - core

    def slot_of(step, whose):
        return lax.rem(z + step + nz, nz) * 2 + whose

    for c in range(NCH):
        hop(ep, c, up_ep).start()
        hop(ep, c, dn_ep).start()
        hand(ep, c).start()

    def flash(slots_in, diagonal=False):
        top, got = (None, None) if diagonal else (mx_run[...], acc[...])
        halves = [
            [jnp.concatenate([kv[i, h * NH + c] for c in range(NH)], axis=1) for h in range(2)]
            for i in slots_in
        ]
        scores = [[dot(p[0:KR], qa[...], ((0,), (0,))) for p in pair] for pair in halves]
        for pair, s in zip(halves, scores):
            if diagonal:
                s = [
                    jnp.where(
                        iota((half_t, tq), 0) + h * half_t <= iota((half_t, tq), 1), s[h], -1e30
                    )
                    for h in range(2)
                ]
            new = jnp.maximum(
                jnp.max(s[0], axis=0, keepdims=True), jnp.max(s[1], axis=0, keepdims=True)
            )
            if top is not None:
                new = jnp.maximum(top, new)
                got = got * jnp.exp(top - new)
            w = [jnp.exp(p - new).astype(BF16) for p in s]
            o = dot(
                jnp.concatenate([p[HD:] for p in pair], axis=1), jnp.concatenate(w, axis=0)
            )
            got = o if got is None else got + o
            top = new
        acc[...] = got
        mx_run[...] = top

    loads[13].wait()
    lax.fori_loop(1, n_tp, give_weights, 0)
    wdn[tp] = wd[:, pl.ds(pl.multiple_of(tp * 128, 128), 128)]
    flash([ep], diagonal=True)

    def take(one, other):
        @pl.when(jnp.maximum(one, other) < ep)
        def _():
            flash([one, other])

        @pl.when(jnp.logical_and(jnp.minimum(one, other) < ep, jnp.maximum(one, other) >= ep))
        def _():
            flash([jnp.minimum(one, other)])

    def wait_piece(slot, c):
        hop(slot, c, up_ep).wait_recv()

    def wait_block(slot):
        sem = far_recv.at[lax.div(slot, 2)]
        send(kv.at[slot], kv.at[slot], kv_send, sem, sib_ep, tp).wait_recv()

    t0, t1 = Torus(0, ep, tp), Torus(1, ep, tp)
    rows = g0.shape[1]
    mg = [
        Gather(t0, g0, rows // 2, mg_s.at[0], mg_r.at[0]),
        Gather(t1, g1, rows // 2, mg_s.at[1], mg_r.at[1]),
    ]
    mh = [
        Gather(t0, h0, fh // 4, mh_s.at[0], mh_r.at[0]),
        Gather(t1, h1, fh // 4, mh_s.at[1], mh_r.at[1]),
    ]
    tiles = range(SIDE * SIDE)
    places = [list(tiles), [SIDE * (t % SIDE) + t // SIDE for t in tiles]]
    returns = Exchange(ep, tp, n_ep, cap, retb, backb, b_s, b_r)

    def pick(rows_out, rows_in, wide_first):
        wide, dense = (0, 1) if wide_first else (1, 0)
        w, d = iota((rows_out, rows_in), wide), iota((rows_out, rows_in), dense)
        i = lax.rem(w, SLOT)
        hit = jnp.logical_and(lax.div(w, SLOT) * cap + i == d, i < cap)
        return hit.astype(F32).astype(BF16)

    def pack_rows():
        dispatch.arrive()
        packed = dot(
            pick(2 * rows, slots, False), recvb[...].reshape(slots, 128)
        ).astype(BF16)
        mg[0].put(packed[:rows])
        mg[1].put(packed[rows:])
        for m in mg:
            m.stage(0)

    def experts_now():
        for d in loads[11:13]:
            d.wait()
        for m in mg:
            m.stage(4)
        wide = jnp.concatenate(
            [
                jnp.concatenate([buf[i] for i in place], axis=1)
                for buf, place in zip((g0, g1), places)
            ],
            axis=0,
        )
        sums = dot(wgu[...], wide, ((1,), (1,)))
        gs, us = sums[:fh], sums[fh:]
        hidden = (gs / (1.0 + jnp.exp(-gs)) * us).astype(BF16)
        mh[0].put(hidden[: fh // 2])
        mh[1].put(hidden[fh // 2 :])
        for m in mh:
            m.stage(0)

    def give_back():
        take_weights()
        for m in mh:
            m.stage(4)
        tall = jnp.concatenate(
            [
                buf[i] for both in zip(*places) for buf, i in zip((h0, h1), both)
            ],
            axis=0,
        )
        rows_out = dot(wdn[...].reshape(n_tp * fh, 128), tall, ((0,), (0,))).astype(BF16)
        retb[...] = (
            dot(pick(slots, 2 * rows, True), rows_out, ((1,), (1,)))
            .astype(BF16)
            .reshape(n_ep, SLOT, 128)
        )
        returns.start()

    hooks = {
        (1, 0): pack_rows,
        (2, 0): lambda: [m.stage(1) for m in mg],
        (3, 0): lambda: [m.stage(2) for m in mg],
        (4, 1): lambda: [m.stage(3) for m in mg],
        (5, 1): experts_now,
        (6, 2): lambda: [m.stage(1) for m in mh],
        (7, 2): lambda: [m.stage(2) for m in mh],
        (8, 2): lambda: [m.stage(3) for m in mh],
    }

    def run_hooks(s, part):
        for (at, which), hook in hooks.items():
            if which == part:

                @pl.when(s == at)
                def _():
                    hook()

    def ring(s, _):
        up, dn = slot_of(-s, core), slot_of(s, core)
        for c in range(NCH):
            wait_piece(up, c)

            @pl.when(s < ups)
            def _():
                hop(up, c, up_ep).start()

            hand(up, c).start()

            @pl.when(s <= dns)
            def _():
                wait_piece(dn, c)

                @pl.when(s < dns)
                def _():
                    hop(dn, c, dn_ep).start()

                hand(dn, c).start()

            if c == 1:
                ring_up, ring_dn = slot_of(1 - s, core), slot_of(s - 1, core)
                take(*(lax.select(s >= 2, i, n_ep) for i in (ring_up, ring_dn)))
            elif c == 3:
                far_up, far_dn = slot_of(1 - s, 1 - core), slot_of(s - 1, 1 - core)
                wait_block(far_up)

                @pl.when(s >= 2)
                def _():
                    wait_block(far_dn)

                take(far_up, lax.select(s >= 2, far_dn, n_ep))
            run_hooks(s, c)
        return 0

    lax.fori_loop(1, ups + 1, ring, 0)
    last = slot_of(-ups, 1 - core)
    wait_block(last)
    take(slot_of(-ups, core), last)

    loads[15].wait()
    att = acc[GR:, :] / acc[3:4, :]
    head = norm_cols(att, to_col(h_gain[...])).astype(BF16)
    hg = [
        Gather(t0, hg0, HD // 2, hg_s.at[0], hg_r.at[0]),
        Gather(t1, hg1, HD // 2, hg_s.at[1], hg_r.at[1]),
    ]
    for i, m in enumerate(hg):
        m.put(head[:, i * half_t : (i + 1) * half_t])
        m.stage(0)
    for m in hg:
        m.stage(1)
    give_back()
    for m in hg:
        m.stage(2)
    for m in hg:
        m.stage(3)
    loads[14].wait()
    loads[16].wait()
    for i, (m, buf) in enumerate(((hg[0], hg0), (hg[1], hg1))):
        m.stage(4)
        tall = jnp.concatenate([buf[j] for j in places[i]], axis=0)
        o = dot(tall, wo[...], ((0,), (0,)))
        mixer_out[i * half_t : (i + 1) * half_t, :] = o.astype(BF16)

    returns.arrive()
    back = backb[...].reshape(slots, 128)
    total = None
    for k in range(2):
        got = dot(onehot[k], back, ((0,), (0,))) * to_col(rweight[k : k + 1, :])
        total = got if total is None else total + got
    moe_out[...] = total.astype(BF16)

    most = kv.at[pl.ds(0, n_ep - 1)]
    send(most, most, kv_send, far_recv.at[z], sib_ep, tp).wait_send()


def body(
    n_ep,
    n_tp,
    attn_in,
    mix_gain,
    query_weight,
    key_weight,
    value_weight,
    query_gain,
    key_gain,
    log_cache,
    head_gain,
    out_weight,
    moe_in,
    moe_gain,
    routes,
    route_weight,
    expert_gate,
    expert_up,
    expert_down,
):
    tq, d = attn_in.shape
    toks = moe_in.shape[0]
    fh = expert_down.shape[1]
    cap = 3 * toks * routes.shape[1] // (2 * n_ep)
    rows = n_ep * cap // 2
    vm = pl.BlockSpec(memory_space=pltpu.VMEM)
    hbm = pl.BlockSpec(memory_space=pl.ANY)
    dma = pltpu.SemaphoreType.DMA

    def v(*shape, dtype=BF16):
        return pltpu.VMEM(shape, dtype)

    nz = n_ep // 2
    scratch = [
        v(tq, d),
        v(tq, d),
        v(3 * HD, d),
        v(n_tp * HD, 128),
        v(toks, d),
        v(2 * fh, d),
        v(fh, d),
        v(n_ep, NCH, BR, tq // NCH),
        v(KR, tq),
        v(GR + HD, tq, dtype=F32),
        v(1, tq, dtype=F32),
        v(n_tp, HD, tq // 2),
        v(n_tp, HD, tq // 2),
        v(n_ep, SLOT, 128),
        v(n_ep, SLOT, 128),
        v(n_ep, SLOT, 128),
        v(n_ep, SLOT, 128),
        v(2, n_ep * SLOT, toks),
        v(n_tp, rows, 128),
        v(n_tp, rows, 128),
        v(n_tp, fh // 2, 2 * rows),
        v(n_tp, fh // 2, 2 * rows),
        v(n_tp, fh, 128),
        v(1, d, dtype=F32),
        v(1, HD, dtype=F32),
        v(1, HD, dtype=F32),
        v(1, tq, dtype=F32),
        v(1, HD, dtype=F32),
        v(1, d, dtype=F32),
        v(2, toks, dtype=jnp.int32),
        v(2, toks, dtype=F32),
        dma((17,)),
        dma((nz, NCH)),
        dma((nz,)),
        dma,
        dma((2,)),
        dma((2, 6)),
        dma((2,)),
        dma((2, 6)),
        dma((2,)),
        dma((2, 6)),
        dma,
        dma,
        dma,
        dma,
        dma,
        dma,
    ]
    return pl.pallas_call(
        functools.partial(kernel, n_ep, n_tp),
        out_shape=(
            jax.ShapeDtypeStruct((tq, 128), BF16),
            jax.ShapeDtypeStruct((toks, 128), BF16),
        ),
        in_specs=[hbm] * 17,
        out_specs=(vm, vm),
        scratch_shapes=scratch,
        compiler_params=pltpu.CompilerParams(
            collective_id=0, has_side_effects=True, vmem_limit_bytes=60 * 1024 * 1024
        ),
    )(
        attn_in,
        mix_gain.reshape(1, -1),
        query_weight.T,
        key_weight.T,
        value_weight.T,
        query_gain.reshape(1, -1),
        key_gain.reshape(1, -1),
        log_cache.reshape(1, -1),
        head_gain.reshape(1, -1),
        out_weight,
        moe_in,
        moe_gain.reshape(1, -1),
        routes.T,
        route_weight.T,
        jnp.swapaxes(expert_gate, 1, 2),
        jnp.swapaxes(expert_up, 1, 2),
        expert_down,
    )


def solution(mesh):
    n_ep, n_tp = mesh.shape["ep"], mesh.shape["tp"]
    in_specs = (
        P("ep", None),
        P(),
        P(None, "tp"),
        P(None, "tp"),
        P(None, "tp"),
        P(),
        P(),
        P("ep", "tp"),
        P("tp"),
        P(None, "tp"),
        P("ep", None),
        P(),
        P("ep", None),
        P("ep", None),
        P("ep", None, "tp"),
        P("ep", None, "tp"),
        P("ep", "tp", None),
    )
    out_specs = (P("ep", "tp"), P("ep", "tp"))
    return jax.shard_map(
        functools.partial(body, n_ep, n_tp),
        mesh=mesh,
        in_specs=in_specs,
        out_specs=out_specs,
        check_vma=False,
    )
```

time: 107 us -> 80.9 us (0.76)
  Pallas kernels: 92.5 us -> 77.1 us
  local copies, waits for them, and re-layouts: 13.7 us -> 2.94 us
    pallas_call x1, Pallas kernels: 92.5 us -> 77.1 us  [body(): pl.pallas_call(functools.partial(kernel, n_ep, n_tp), out_shape=(jax.Shap...]
    unnamed x13 -> x2, local copies, waits for them, and re-layouts: 13.7 us -> 2.94 us
where the time goes in v2:
time: 80.9 us; the launch traced here: 80.7 us
  Pallas kernels  77.1 us (95%)
  local copies, waits for them, and re-layouts  2.94 us (4%)
    pallas_call x1, Pallas kernels, body(): pl.pallas_call(functools.partial(kernel, n_ep, n_tp), out_shape=(jax.Shap...  77.1 us
    unnamed x2, local copies, waits for them, and re-layouts  2.94 us

profile of v2, /device:TPU:1, one launch (start us, length us, event | category | flops | bytes accessed | tf_op | source)
XLA Modules:
  0.0 80.7 jit_solution(16872100110509850472)
XLA Ops:
  0.6 77.1 %shard_map.176 = (bf16[512,128]{1,0:T(8,128)(2,1)}, bf16[128,128]{1,0:T(8,128)(2,1)}) custom-call(bf16[512,2048]{1,0:T(8,128)(2,1)} %x_h.1, f32[1,2048]{1,0:T(1,128)} %bitcast.18, bf16[64,2048]{1,0:T(8,128)(2,1)} %bitcast.13, bf16[64,2048]{1,0:T(8,128)(2,1)} %bitcast.14, bf16[64,2048]{1,0:T(8,128)(2,1)} %bitcast.15, f32[1,64]{1,0:T(1,128)} %bitcast.23, ...), custom_call_target="tpu_custom_call" | custom-call | tf_op jit(solution)/shard_map/pallas_call | solution.py:683
  77.7 1.6 %copy.21 = bf16[512,128]{1,0:T(8,128)(2,1)} copy(bf16[512,128]{1,0:T(8,128)(2,1)} %get-tuple-element.4) | data formatting | bytes 262144
  79.3 1.4 %copy.22 = bf16[128,128]{1,0:T(8,128)(2,1)} copy(bf16[128,128]{1,0:T(8,128)(2,1)} %get-tuple-element.5) | data formatting | bytes 65536

commit v3 on v2

--- a/solution.py
+++ b/solution.py
@@ -16,6 +16,7 @@
 SLOT = 16
 NCH = 4
 NH = NCH // 2
+DISPATCH_AFTER = 0
 MESH = pl.DeviceIdType.MESH
 F32 = jnp.float32
 BF16 = jnp.bfloat16
@@ -98,15 +99,10 @@
         if k == 0:
             self.go(a, b, self.right_b, 0)
             self.go(a, b, self.left_b, 0)
-            self.go(a, b, self.right_a, 2)
-            self.go(a, b, self.left_a, 2)
         elif k == 1:
             self.got(0, 2)
             self.go(a, self.bm, self.right_b, 1, self.lo)
             self.go(a, self.bp, self.left_b, 1, self.hi)
-            for j in (self.bm, self.bp):
-                self.go(a, j, self.right_a, 3)
-                self.go(a, j, self.left_a, 3)
         elif k == 2:
             self.got(1, 1)
             self.go(a, self.bo, self.right_a, 4)
@@ -122,6 +118,23 @@
         else:
             self.got(5, 4)
             self.whole(SIDE * SIDE - 1, 5).wait_send()
+
+    def across(self, k):
+        a, b = self.t.a, self.t.b
+        if k == 0:
+            self.go(a, b, self.right_a, 2)
+            self.go(a, b, self.left_a, 2)
+        elif k == 1:
+            for j in (self.bm, self.bp):
+                self.go(a, j, self.right_a, 3)
+                self.go(a, j, self.left_a, 3)
+
+
+def step_all(gathers, k):
+    for m in gathers:
+        m.stage(k)
+    for m in gathers:
+        m.across(k)
 
 
 class Exchange:
@@ -188,6 +201,10 @@
     nx,
     wqkv,
     wo,
+    wot,
+    wdt,
+    to_dense,
+    to_wide,
     mx,
     wgu,
     wd,
@@ -241,13 +258,14 @@
     fh = wd.shape[0]
     cap = 2 * g0.shape[1] // n_ep
 
-    recvb[...] = jnp.zeros_like(recvb)
-    backb[...] = jnp.zeros_like(backb)
     barrier = pltpu.get_barrier_semaphore()
+
+    def far_first(i):
+        return n_ep // 2 + lax.select(lax.rem(i, 2) == 1, lax.div(i, 2), -lax.div(i, 2))
 
     def greet_ep(i, _):
         pl.semaphore_signal(
-            barrier, inc=1, device_id=(lax.rem(ep + i, n_ep), tp), device_id_type=MESH
+            barrier, inc=1, device_id=(lax.rem(ep + far_first(i), n_ep), tp), device_id_type=MESH
         )
         return 0
 
@@ -341,10 +359,20 @@
         kv[ep, c, HD:KR, :] = grow[:, cc]
         kv[ep, c, KR:BR, :] = vt[:, cc]
 
+    def pick(rows_out, rows_in, wide_first):
+        wide, dense = (0, 1) if wide_first else (1, 0)
+        w, d = iota((rows_out, rows_in), wide), iota((rows_out, rows_in), dense)
+        i = lax.rem(w, SLOT)
+        hit = jnp.logical_and(lax.div(w, SLOT) * cap + i == d, i < cap)
+        return hit.astype(F32).astype(BF16)
+
+    to_dense[...] = pick(2 * g0.shape[1], slots, False)
+    to_wide[...] = pick(slots, 2 * g0.shape[1], True)
+    loads[14].wait()
+    wot[...] = wo[...].astype(F32).T.astype(BF16)
     pl.semaphore_wait(barrier, n_ep - 1 + n_tp - 1)
 
     dispatch = Exchange(ep, tp, n_ep, cap, sendb, recvb, d_s, d_r)
-    dispatch.start()
 
     def features(t):
         return wd.at[:, pl.ds(pl.multiple_of(t * 128, 128), 128)]
@@ -379,6 +407,8 @@
         hop(ep, c, up_ep).start()
         hop(ep, c, dn_ep).start()
         hand(ep, c).start()
+        if c == DISPATCH_AFTER:
+            dispatch.start()
 
     def flash(slots_in, diagonal=False):
         top, got = (None, None) if diagonal else (mx_run[...], acc[...])
@@ -445,28 +475,25 @@
     places = [list(tiles), [SIDE * (t % SIDE) + t // SIDE for t in tiles]]
     returns = Exchange(ep, tp, n_ep, cap, retb, backb, b_s, b_r)
 
-    def pick(rows_out, rows_in, wide_first):
-        wide, dense = (0, 1) if wide_first else (1, 0)
-        w, d = iota((rows_out, rows_in), wide), iota((rows_out, rows_in), dense)
-        i = lax.rem(w, SLOT)
-        hit = jnp.logical_and(lax.div(w, SLOT) * cap + i == d, i < cap)
-        return hit.astype(F32).astype(BF16)
+    def filled(buf):
+        used = iota((n_ep, SLOT, 128), 1) < cap
+        return jnp.where(used, buf[...].astype(F32), 0.0).astype(BF16).reshape(slots, 128)
 
     def pack_rows():
         dispatch.arrive()
         packed = dot(
-            pick(2 * rows, slots, False), recvb[...].reshape(slots, 128)
+            to_dense[...], filled(recvb)
         ).astype(BF16)
         mg[0].put(packed[:rows])
         mg[1].put(packed[rows:])
-        for m in mg:
-            m.stage(0)
+        step_all(mg, 0)
 
     def experts_now():
         for d in loads[11:13]:
             d.wait()
-        for m in mg:
-            m.stage(4)
+        take_weights()
+        wdt[...] = wdn[...].reshape(n_tp * fh, 128).astype(F32).T.astype(BF16)
+        step_all(mg, 4)
         wide = jnp.concatenate(
             [
                 jnp.concatenate([buf[i] for i in place], axis=1)
@@ -479,41 +506,38 @@
         hidden = (gs / (1.0 + jnp.exp(-gs)) * us).astype(BF16)
         mh[0].put(hidden[: fh // 2])
         mh[1].put(hidden[fh // 2 :])
-        for m in mh:
-            m.stage(0)
+        step_all(mh, 0)
 
     def give_back():
-        take_weights()
-        for m in mh:
-            m.stage(4)
+        step_all(mh, 4)
         tall = jnp.concatenate(
             [
                 buf[i] for both in zip(*places) for buf, i in zip((h0, h1), both)
             ],
             axis=0,
         )
-        rows_out = dot(wdn[...].reshape(n_tp * fh, 128), tall, ((0,), (0,))).astype(BF16)
+        rows_out = dot(wdt[...], tall).astype(BF16)
         retb[...] = (
-            dot(pick(slots, 2 * rows, True), rows_out, ((1,), (1,)))
+            dot(to_wide[...], rows_out, ((1,), (1,)))
             .astype(BF16)
             .reshape(n_ep, SLOT, 128)
         )
         returns.start()
 
     hooks = {
-        (1, 0): pack_rows,
-        (2, 0): lambda: [m.stage(1) for m in mg],
-        (3, 0): lambda: [m.stage(2) for m in mg],
-        (4, 1): lambda: [m.stage(3) for m in mg],
-        (5, 1): experts_now,
-        (6, 2): lambda: [m.stage(1) for m in mh],
-        (7, 2): lambda: [m.stage(2) for m in mh],
-        (8, 2): lambda: [m.stage(3) for m in mh],
+        (1, 3): pack_rows,
+        (2, 3): lambda: step_all(mg, 1),
+        (4, 0): lambda: step_all(mg, 2),
+        (5, 0): lambda: step_all(mg, 3),
+        (6, 0): experts_now,
+        (7, 0): lambda: step_all(mh, 1),
+        (8, 0): lambda: step_all(mh, 2),
+        (9, 0): lambda: step_all(mh, 3),
     }
 
     def run_hooks(s, part):
         for (at, which), hook in hooks.items():
-            if which == part:
+            if which == part and at <= ups:
 
                 @pl.when(s == at)
                 def _():
@@ -524,7 +548,7 @@
         for c in range(NCH):
             wait_piece(up, c)
 
-            @pl.when(s < ups)
+            @pl.when(s < (ups if c < NH else dns))
             def _():
                 hop(up, c, up_ep).start()
 
@@ -534,7 +558,7 @@
             def _():
                 wait_piece(dn, c)
 
-                @pl.when(s < dns)
+                @pl.when(s < (dns if c < NH else ups))
                 def _():
                     hop(dn, c, dn_ep).start()
 
@@ -569,24 +593,26 @@
     ]
     for i, m in enumerate(hg):
         m.put(head[:, i * half_t : (i + 1) * half_t])
-        m.stage(0)
-    for m in hg:
-        m.stage(1)
+    step_all(hg, 0)
+    for (at, _), hook in hooks.items():
+        if at == ups + 1:
+            hook()
+    step_all(hg, 1)
     give_back()
-    for m in hg:
-        m.stage(2)
-    for m in hg:
-        m.stage(3)
-    loads[14].wait()
+    for (at, _), hook in hooks.items():
+        if at == ups + 2:
+            hook()
+    step_all(hg, 2)
+    step_all(hg, 3)
     loads[16].wait()
     for i, (m, buf) in enumerate(((hg[0], hg0), (hg[1], hg1))):
         m.stage(4)
         tall = jnp.concatenate([buf[j] for j in places[i]], axis=0)
-        o = dot(tall, wo[...], ((0,), (0,)))
-        mixer_out[i * half_t : (i + 1) * half_t, :] = o.astype(BF16)
+        o = dot(wot[...], tall)
+        mixer_out[i * half_t : (i + 1) * half_t, :] = o.T.astype(BF16)
 
     returns.arrive()
-    back = backb[...].reshape(slots, 128)
+    back = filled(backb)
     total = None
     for k in range(2):
         got = dot(onehot[k], back, ((0,), (0,))) * to_col(rweight[k : k + 1, :])
@@ -636,6 +662,10 @@
         v(tq, d),
         v(3 * HD, d),
         v(n_tp * HD, 128),
+        v(128, n_tp * HD),
+        v(128, n_tp * fh),
+        v(2 * rows, n_ep * SLOT),
+        v(n_ep * SLOT, 2 * rows),
         v(toks, d),
         v(2 * fh, d),
         v(fh, d),
@@ -683,8 +713,8 @@
     return pl.pallas_call(
         functools.partial(kernel, n_ep, n_tp),
         out_shape=(
-            jax.ShapeDtypeStruct((tq, 128), BF16),
-            jax.ShapeDtypeStruct((toks, 128), BF16),
+            pltpu.VMEM((tq, 128), BF16),
+            pltpu.VMEM((toks, 128), BF16),
         ),
         in_specs=[hbm] * 17,
         out_specs=(vm, vm),

time: 80.9 us -> 73.4 us (0.907)
  Pallas kernels: 77.1 us -> 71.4 us
  local copies, waits for them, and re-layouts: 2.94 us -> 1.27 us
    pallas_call x1, Pallas kernels: 77.1 us -> 71.4 us  [body(): pl.pallas_call(functools.partial(kernel, n_ep, n_tp), out_shape=(pltpu.VM...]
    unnamed x2, local copies, waits for them, and re-layouts: 2.94 us -> 1.27 us
where the time goes in v3:
time: 73.4 us; the launch traced here: 73.3 us
  Pallas kernels  71.4 us (97%)
  local copies, waits for them, and re-layouts  1.27 us (2%)
    pallas_call x1, Pallas kernels, body(): pl.pallas_call(functools.partial(kernel, n_ep, n_tp), out_shape=(pltpu.VM...  71.4 us

profile of v3, /device:TPU:1, one launch (start us, length us, event | category | flops | bytes accessed | tf_op | source)
XLA Modules:
  0.0 73.3 jit_solution(3548415738114460996)
XLA Ops:
  0.6 71.4 %shard_map.176 = (bf16[512,128]{1,0:T(8,128)(2,1)S(1)}, bf16[128,128]{1,0:T(8,128)(2,1)S(1)}) custom-call(bf16[512,2048]{1,0:T(8,128)(2,1)} %x_h.1, f32[1,2048]{1,0:T(1,128)} %bitcast.18, bf16[64,2048]{1,0:T(8,128)(2,1)} %bitcast.13, bf16[64,2048]{1,0:T(8,128)(2,1)} %bitcast.14, bf16[64,2048]{1,0:T(8,128)(2,1)} %bitcast.15, f32[1,64]{1,0:T(1,128)} %bitcast.23, ...), custom_call_target="tpu_custom_call" | custom-call | tf_op jit(solution)/shard_map/pallas_call | solution.py:713
  72.0 0.7 copy.21
  72.7 0.6 copy.22

commit v4 on v3

--- a/solution.py
+++ b/solution.py
@@ -71,20 +71,20 @@
 
 
 class Gather:
-    def __init__(self, torus, buf, half, ssem, rsem):
+    def __init__(self, torus, buf, ssem, rsem):
         self.t, self.buf, self.ss, self.rs = torus, buf, ssem, rsem
         a, b = torus.a, torus.b
         self.am, self.ap = (lax.rem(a + k, SIDE) for k in (3, 1))
         self.bm, self.bp, self.bo = (lax.rem(b + k, SIDE) for k in (3, 1, 2))
-        self.lo, self.hi = pl.ds(0, half), pl.ds(half, half)
+        self.across_b = torus.at(a, b + 2)
         self.right_b, self.left_b = torus.at(a, b + 1), torus.at(a, b - 1)
         self.right_a, self.left_a = torus.at(a + 1, b), torus.at(a - 1, b)
 
     def put(self, block):
         self.buf[SIDE * self.t.a + self.t.b] = block
 
-    def go(self, a, b, to, k, rows=slice(None)):
-        src = self.buf.at[SIDE * a + b, rows]
+    def go(self, a, b, to, k):
+        src = self.buf.at[SIDE * a + b]
         send(src, src, self.ss, self.rs.at[k], self.t.ep, to).start()
 
     def whole(self, n, k):
@@ -97,44 +97,38 @@
     def stage(self, k):
         a, b = self.t.a, self.t.b
         if k == 0:
+            self.go(a, b, self.across_b, 0)
             self.go(a, b, self.right_b, 0)
             self.go(a, b, self.left_b, 0)
         elif k == 1:
-            self.got(0, 2)
-            self.go(a, self.bm, self.right_b, 1, self.lo)
-            self.go(a, self.bp, self.left_b, 1, self.hi)
+            self.got(0, 3)
         elif k == 2:
-            self.got(1, 1)
-            self.go(a, self.bo, self.right_a, 4)
-            self.go(a, self.bo, self.left_a, 4)
-            self.got(2, 2)
-            self.go(self.am, b, self.right_a, 5)
+            self.got(1, 2)
+            self.go(self.am, b, self.right_a, 3)
+            self.got(2, 6)
+            self.go(self.am, self.bm, self.right_a, 3)
+            self.go(self.ap, self.bp, self.left_a, 3)
+            self.go(self.ap, self.bo, self.left_a, 3)
+        else:
             self.got(3, 4)
-            self.go(self.am, self.bm, self.right_a, 5)
-            self.go(self.ap, self.bp, self.left_a, 5)
-        elif k == 3:
-            self.got(4, 2)
-            self.go(self.ap, self.bo, self.left_a, 5)
-        else:
-            self.got(5, 4)
-            self.whole(SIDE * SIDE - 1, 5).wait_send()
-
-    def across(self, k):
+            self.whole(SIDE * SIDE - 1, 3).wait_send()
+
+    def second(self, k):
         a, b = self.t.a, self.t.b
         if k == 0:
-            self.go(a, b, self.right_a, 2)
-            self.go(a, b, self.left_a, 2)
+            self.go(a, b, self.right_a, 1)
+            self.go(a, b, self.left_a, 1)
         elif k == 1:
-            for j in (self.bm, self.bp):
-                self.go(a, j, self.right_a, 3)
-                self.go(a, j, self.left_a, 3)
+            for j in (self.bm, self.bp, self.bo):
+                self.go(a, j, self.right_a, 2)
+                self.go(a, j, self.left_a, 2)
 
 
 def step_all(gathers, k):
     for m in gathers:
         m.stage(k)
     for m in gathers:
-        m.across(k)
+        m.second(k)
 
 
 class Exchange:
@@ -464,12 +458,12 @@
     t0, t1 = Torus(0, ep, tp), Torus(1, ep, tp)
     rows = g0.shape[1]
     mg = [
-        Gather(t0, g0, rows // 2, mg_s.at[0], mg_r.at[0]),
-        Gather(t1, g1, rows // 2, mg_s.at[1], mg_r.at[1]),
+        Gather(t0, g0, mg_s.at[0], mg_r.at[0]),
+        Gather(t1, g1, mg_s.at[1], mg_r.at[1]),
     ]
     mh = [
-        Gather(t0, h0, fh // 4, mh_s.at[0], mh_r.at[0]),
-        Gather(t1, h1, fh // 4, mh_s.at[1], mh_r.at[1]),
+        Gather(t0, h0, mh_s.at[0], mh_r.at[0]),
+        Gather(t1, h1, mh_s.at[1], mh_r.at[1]),
     ]
     tiles = range(SIDE * SIDE)
     places = [list(tiles), [SIDE * (t % SIDE) + t // SIDE for t in tiles]]
@@ -493,7 +487,7 @@
             d.wait()
         take_weights()
         wdt[...] = wdn[...].reshape(n_tp * fh, 128).astype(F32).T.astype(BF16)
-        step_all(mg, 4)
+        step_all(mg, 3)
         wide = jnp.concatenate(
             [
                 jnp.concatenate([buf[i] for i in place], axis=1)
@@ -509,7 +503,7 @@
         step_all(mh, 0)
 
     def give_back():
-        step_all(mh, 4)
+        step_all(mh, 3)
         tall = jnp.concatenate(
             [
                 buf[i] for both in zip(*places) for buf, i in zip((h0, h1), both)
@@ -526,13 +520,11 @@
 
     hooks = {
         (1, 3): pack_rows,
-        (2, 3): lambda: step_all(mg, 1),
-        (4, 0): lambda: step_all(mg, 2),
-        (5, 0): lambda: step_all(mg, 3),
+        (3, 0): lambda: step_all(mg, 1),
+        (4, 2): lambda: step_all(mg, 2),
         (6, 0): experts_now,
-        (7, 0): lambda: step_all(mh, 1),
-        (8, 0): lambda: step_all(mh, 2),
-        (9, 0): lambda: step_all(mh, 3),
+        (7, 1): lambda: step_all(mh, 1),
+        (8, 1): lambda: step_all(mh, 2),
     }
 
     def run_hooks(s, part):
@@ -588,25 +580,21 @@
     att = acc[GR:, :] / acc[3:4, :]
     head = norm_cols(att, to_col(h_gain[...])).astype(BF16)
     hg = [
-        Gather(t0, hg0, HD // 2, hg_s.at[0], hg_r.at[0]),
-        Gather(t1, hg1, HD // 2, hg_s.at[1], hg_r.at[1]),
+        Gather(t0, hg0, hg_s.at[0], hg_r.at[0]),
+        Gather(t1, hg1, hg_s.at[1], hg_r.at[1]),
     ]
     for i, m in enumerate(hg):
         m.put(head[:, i * half_t : (i + 1) * half_t])
     step_all(hg, 0)
     for (at, _), hook in hooks.items():
-        if at == ups + 1:
+        if at > ups:
             hook()
+    give_back()
     step_all(hg, 1)
-    give_back()
-    for (at, _), hook in hooks.items():
-        if at == ups + 2:
-            hook()
     step_all(hg, 2)
-    step_all(hg, 3)
     loads[16].wait()
     for i, (m, buf) in enumerate(((hg[0], hg0), (hg[1], hg1))):
-        m.stage(4)
+        m.stage(3)
         tall = jnp.concatenate([buf[j] for j in places[i]], axis=0)
         o = dot(wot[...], tall)
         mixer_out[i * half_t : (i + 1) * half_t, :] = o.T.astype(BF16)
@@ -698,11 +686,11 @@
         dma((nz,)),
         dma,
         dma((2,)),
-        dma((2, 6)),
+        dma((2, 4)),
         dma((2,)),
-        dma((2, 6)),
+        dma((2, 4)),
         dma((2,)),
-        dma((2, 6)),
+        dma((2, 4)),
         dma,
         dma,
         dma,

time: 73.4 us -> 69.3 us (0.944)
  Pallas kernels: 71.4 us -> 67.2 us
    pallas_call x1, Pallas kernels: 71.4 us -> 67.2 us  [body(): pl.pallas_call(functools.partial(kernel, n_ep, n_tp), out_shape=(pltpu.VM...]
where the time goes in v4:
time: 69.3 us; the launch traced here: 69.1 us
  Pallas kernels  67.2 us (97%)
  local copies, waits for them, and re-layouts  1.27 us (2%)
    pallas_call x1, Pallas kernels, body(): pl.pallas_call(functools.partial(kernel, n_ep, n_tp), out_shape=(pltpu.VM...  67.2 us

profile of v4, /device:TPU:1, one launch (start us, length us, event | category | flops | bytes accessed | tf_op | source)
XLA Modules:
  0.0 69.1 jit_solution(7861683730236869839)
XLA Ops:
  0.6 67.2 %shard_map.176 = (bf16[512,128]{1,0:T(8,128)(2,1)S(1)}, bf16[128,128]{1,0:T(8,128)(2,1)S(1)}) custom-call(bf16[512,2048]{1,0:T(8,128)(2,1)} %x_h.1, f32[1,2048]{1,0:T(1,128)} %bitcast.18, bf16[64,2048]{1,0:T(8,128)(2,1)} %bitcast.13, bf16[64,2048]{1,0:T(8,128)(2,1)} %bitcast.14, bf16[64,2048]{1,0:T(8,128)(2,1)} %bitcast.15, f32[1,64]{1,0:T(1,128)} %bitcast.23, ...), custom_call_target="tpu_custom_call" | custom-call | tf_op jit(solution)/shard_map/pallas_call | solution.py:701
  67.9 0.7 copy.21
  68.5 0.6 copy.22

commit v5 on v4

--- a/solution.py
+++ b/solution.py
@@ -105,11 +105,12 @@
         elif k == 2:
             self.got(1, 2)
             self.go(self.am, b, self.right_a, 3)
-            self.got(2, 6)
+            self.got(2, 3)
             self.go(self.am, self.bm, self.right_a, 3)
             self.go(self.ap, self.bp, self.left_a, 3)
             self.go(self.ap, self.bo, self.left_a, 3)
         else:
+            self.got(4, 3)
             self.got(3, 4)
             self.whole(SIDE * SIDE - 1, 3).wait_send()
 
@@ -119,9 +120,12 @@
             self.go(a, b, self.right_a, 1)
             self.go(a, b, self.left_a, 1)
         elif k == 1:
-            for j in (self.bm, self.bp, self.bo):
-                self.go(a, j, self.right_a, 2)
-                self.go(a, j, self.left_a, 2)
+            self.go(a, self.bm, self.right_a, 2)
+            self.go(a, self.bp, self.left_a, 2)
+            self.go(a, self.bo, self.left_a, 2)
+            self.go(a, self.bp, self.right_a, 4)
+            self.go(a, self.bo, self.right_a, 4)
+            self.go(a, self.bm, self.left_a, 4)
 
 
 def step_all(gathers, k):
@@ -686,11 +690,11 @@
         dma((nz,)),
         dma,
         dma((2,)),
-        dma((2, 4)),
+        dma((2, 5)),
         dma((2,)),
-        dma((2, 4)),
+        dma((2, 5)),
         dma((2,)),
-        dma((2, 4)),
+        dma((2, 5)),
         dma,
         dma,
         dma,

time: 69.3 us -> 68.7 us (level)
  no operation moved by 1% of the time
where the time goes in v5:
time: 68.7 us; the launch traced here: 68.6 us
  Pallas kernels  66.6 us (97%)
  local copies, waits for them, and re-layouts  1.27 us (2%)
    pallas_call x1, Pallas kernels, body(): pl.pallas_call(functools.partial(kernel, n_ep, n_tp), out_shape=(pltpu.VM...  66.6 us

profile of v5, /device:TPU:1, one launch (start us, length us, event | category | flops | bytes accessed | tf_op | source)
XLA Modules:
  0.0 68.6 jit_solution(12433412674883320209)
XLA Ops:
  0.6 66.6 %shard_map.176 = (bf16[512,128]{1,0:T(8,128)(2,1)S(1)}, bf16[128,128]{1,0:T(8,128)(2,1)S(1)}) custom-call(bf16[512,2048]{1,0:T(8,128)(2,1)} %x_h.1, f32[1,2048]{1,0:T(1,128)} %bitcast.18, bf16[64,2048]{1,0:T(8,128)(2,1)} %bitcast.13, bf16[64,2048]{1,0:T(8,128)(2,1)} %bitcast.14, bf16[64,2048]{1,0:T(8,128)(2,1)} %bitcast.15, f32[1,64]{1,0:T(1,128)} %bitcast.23, ...), custom_call_target="tpu_custom_call" | custom-call | tf_op jit(solution)/shard_map/pallas_call | solution.py:705
  67.3 0.7 copy.21
  67.9 0.6 copy.22

commit v6 on v5

--- a/solution.py
+++ b/solution.py
@@ -145,7 +145,8 @@
         self.dst[self.ep] = self.src[self.ep]
 
         def one(i, _):
-            step = lax.select(lax.rem(i, 2) == 1, lax.div(i + 1, 2), self.n - lax.div(i, 2))
+            off = lax.div(i, 2)
+            step = self.n // 2 + lax.select(lax.rem(i, 2) == 1, off, -off)
             peer = lax.rem(self.ep + step, self.n)
             send(
                 self.src.at[peer, self.used],

time: 68.7 us -> 68.4 us (level)
  no operation moved by 1% of the time
where the time goes in v6:
time: 68.4 us; the launch traced here: 68.2 us
  Pallas kernels  66.3 us (97%)
  local copies, waits for them, and re-layouts  1.27 us (2%)
    pallas_call x1, Pallas kernels, body(): pl.pallas_call(functools.partial(kernel, n_ep, n_tp), out_shape=(pltpu.VM...  66.3 us

profile of v6, /device:TPU:1, one launch (start us, length us, event | category | flops | bytes accessed | tf_op | source)
XLA Modules:
  0.0 68.2 jit_solution(7066130496256937823)
XLA Ops:
  0.6 66.3 %shard_map.176 = (bf16[512,128]{1,0:T(8,128)(2,1)S(1)}, bf16[128,128]{1,0:T(8,128)(2,1)S(1)}) custom-call(bf16[512,2048]{1,0:T(8,128)(2,1)} %x_h.1, f32[1,2048]{1,0:T(1,128)} %bitcast.18, bf16[64,2048]{1,0:T(8,128)(2,1)} %bitcast.13, bf16[64,2048]{1,0:T(8,128)(2,1)} %bitcast.14, bf16[64,2048]{1,0:T(8,128)(2,1)} %bitcast.15, f32[1,64]{1,0:T(1,128)} %bitcast.23, ...), custom_call_target="tpu_custom_call" | custom-call | tf_op jit(solution)/shard_map/pallas_call | solution.py:706
  67.0 0.7 copy.21
  67.6 0.6 copy.22
